TPU v7x, 32 devices: a whole 2x2x4 slice. The times are simulated.
32 devices in a mesh: ep: 16 (over z, y, core), tp: 2 (over x).
Axes of the slice: x: 2, y: 2, z: 4, core: 2. Of those that a mesh axis runs over, the one named last changes fastest.
Arguments:
- tokens: bfloat16 [128, 1024], P('ep'), may hold values from -6 to 6
- ssm_state: float32 [128, 32, 64, 128], P('ep', 'tp'), may hold values from -6 to 6
- conv_x: bfloat16 [128, 3, 2048], P('ep', None, 'tp'), may hold values from -6 to 6
- conv_b: bfloat16 [128, 3, 1024], P('ep', None, 'tp'), may hold values from -6 to 6
- conv_c: bfloat16 [128, 3, 1024], P('ep', None, 'tp'), may hold values from -6 to 6
- w_x: bfloat16 [1024, 2048], P(None, 'tp'), may hold values from -0.1875 to 0.1875
- w_z: bfloat16 [1024, 2048], P(None, 'tp'), may hold values from -0.1875 to 0.1875
- w_b: bfloat16 [1024, 1024], P(None, 'tp'), may hold values from -0.1875 to 0.1875
- w_c: bfloat16 [1024, 1024], P(None, 'tp'), may hold values from -0.1875 to 0.1875
- w_dt: bfloat16 [1024, 32], replicated, may hold values from -0.1875 to 0.1875
- dt_bias: float32 [32], P('tp'), may hold values from -2 to 1
- a_log: float32 [32], P('tp'), may hold values from -3 to 1
- d_skip: float32 [32], P('tp'), may hold values from 0.1 to 1.9
- taps_x: bfloat16 [4, 2048], P(None, 'tp'), may hold values from -3 to 3
- taps_b: bfloat16 [4, 1024], P(None, 'tp'), may hold values from -3 to 3
- taps_c: bfloat16 [4, 1024], P(None, 'tp'), may hold values from -3 to 3
- norm1_gain: float32 [1024], replicated, may hold values from 0.1 to 1.9
- group_gain: float32 [2048], P('tp'), may hold values from 0.1 to 1.9
- w_out: bfloat16 [2048, 1024], P('tp'), may hold values from -0.125 to 0.125
- norm2_gain: float32 [1024], replicated, may hold values from 0.1 to 1.9
- route_ids: int32 [128, 6], P('ep'), may hold values from 0 to 15, all different within a row; in each aligned block of 8 rows (0 to 7, 8 to 15, ...) at most 6 rows name the same one
- route_weights: float32 [128, 6], P('ep'), may hold values from 0.1 to 1
- exp_gate: bfloat16 [16, 1024, 512], P('ep', None, 'tp'), may hold values from -0.1875 to 0.1875
- exp_up: bfloat16 [16, 1024, 512], P('ep', None, 'tp'), may hold values from -0.1875 to 0.1875
- exp_down: bfloat16 [16, 512, 1024], P('ep', 'tp'), may hold values from -0.25 to 0.25
- dense_gate: bfloat16 [1024, 1024], P('ep', 'tp'), may hold values from -0.1875 to 0.1875
- dense_up: bfloat16 [1024, 1024], P('ep', 'tp'), may hold values from -0.1875 to 0.1875
- dense_down: bfloat16 [1024, 1024], P('tp', 'ep'), may hold values from -0.1875 to 0.1875
- branch_gate: bfloat16 [1024], replicated, may hold values from -0.375 to 0.375
Outputs:
- mixed: bfloat16 [128, 1024], P('ep', 'tp')
- state_next: float32 [128, 32, 64, 128], P('ep', 'tp')
- conv_x_next: bfloat16 [128, 3, 2048], P('ep', None, 'tp')
- conv_b_next: bfloat16 [128, 3, 1024], P('ep', None, 'tp')
- conv_c_next: bfloat16 [128, 3, 1024], P('ep', None, 'tp')
Inputs may be any that keep to these rules, and one draw needn't show every extreme that they name: `route_ids`: each row names 6 different experts. Among the rows of one device no expert is named by more than 6 rows, a bound that some block reaches.
All inputs are finite; a program needn't handle non-finite values.
Results may differ from a plain program's by a relative error of at most 0.019.
Values may be sent and summed in bfloat16 or wider, within the bound.
A program may use at most 64 MiB of HBM per device.

v0:
```python
import functools

import jax
import jax.numpy as jnp
from jax import lax
from jax.experimental import pallas as pl
from jax.experimental.pallas import tpu as pltpu
from jax.sharding import PartitionSpec as P

epsilon = 1e-06


def rms_rows(values, gain):
    return values * lax.rsqrt(jnp.mean(values * values, axis=-1, keepdims=True) + epsilon) * gain


def mixer_kernel(
    tokens_ref,
    gain_ref,
    state_hbm,
    prev_x_ref,
    prev_b_ref,
    prev_c_ref,
    wx_hbm,
    wz_hbm,
    wb_hbm,
    wc_hbm,
    wdt_ref,
    bias_ref,
    a_log_ref,
    skip_ref,
    taps_x_ref,
    taps_b_ref,
    taps_c_ref,
    group_gain_ref,
    mixed_ref,
    state_out,
    next_x_ref,
    next_b_ref,
    next_c_ref,
    wx,
    wz,
    wb,
    wc,
    state,
    w_sem,
    in_sem,
    out_sem,
):
    seqs, heads, head_dim, state_dim = state.shape
    groups = wb.shape[1] // state_dim
    per_group = heads // groups
    inner = heads * head_dim
    fetch = [
        pltpu.make_async_copy(hbm, vmem, w_sem.at[i])
        for i, (hbm, vmem) in enumerate(((wx_hbm, wx), (wb_hbm, wb), (wc_hbm, wc), (wz_hbm, wz)))
    ]
    fetch_state = [
        pltpu.make_async_copy(state_hbm.at[s], state.at[s], in_sem.at[s]) for s in range(seqs)
    ]
    put_state = [
        pltpu.make_async_copy(state.at[s], state_out.at[s], out_sem.at[s]) for s in range(seqs)
    ]
    for copy in fetch[:3] + fetch_state + fetch[3:]:
        copy.start()

    def project(weights):
        out = jnp.dot(normed, weights, preferred_element_type=jnp.float32)
        return out.astype(jnp.bfloat16).astype(jnp.float32)

    def conv(prev_ref, fresh, taps_ref, next_ref):
        prev = prev_ref[...].astype(jnp.float32)
        taps = taps_ref[...].astype(jnp.float32)
        depth = prev.shape[0]
        summed = prev[0] * taps[0:1]
        for j in range(1, depth):
            summed = summed + prev[j] * taps[j : j + 1]
            next_ref[j - 1] = prev[j].astype(jnp.bfloat16)
        summed = summed + fresh * taps[depth : depth + 1]
        next_ref[depth - 1] = fresh.astype(jnp.bfloat16)
        return jax.nn.silu(summed)

    normed = rms_rows(tokens_ref[...].astype(jnp.float32), gain_ref[...]).astype(jnp.bfloat16)
    all_dt = lax.dot_general(
        normed, wdt_ref[...], (((1,), (1,)), ((), ())), preferred_element_type=jnp.float32
    )
    dt_raw = all_dt[:, :heads]
    for t in range(1, all_dt.shape[1] // heads):
        own = lax.axis_index("tp") == t
        dt_raw = jnp.where(own, all_dt[:, t * heads : (t + 1) * heads], dt_raw)
    step = jax.nn.softplus(dt_raw + bias_ref[...])
    decay = jnp.exp(-step * jnp.exp(a_log_ref[...]))
    spread = lax.broadcasted_iota(jnp.int32, (heads, inner), 1) // head_dim
    spread = spread == lax.broadcasted_iota(jnp.int32, (heads, inner), 0)
    per_head = jnp.concatenate((step, jnp.broadcast_to(skip_ref[...], step.shape)), axis=0)
    wide = jnp.dot(
        per_head,
        spread.astype(jnp.float32),
        precision=lax.Precision.HIGHEST,
        preferred_element_type=jnp.float32,
    )

    fetch[0].wait()
    xs = conv(prev_x_ref, project(wx[...]), taps_x_ref, next_x_ref)
    fetch[1].wait()
    bs = conv(prev_b_ref, project(wb[...]), taps_b_ref, next_b_ref)
    fetch[2].wait()
    cs = conv(prev_c_ref, project(wc[...]), taps_c_ref, next_c_ref)
    stepped = jnp.transpose(wide[:seqs] * xs)
    cs_high = cs.astype(jnp.bfloat16)
    cs_low = (cs - cs_high.astype(jnp.float32)).astype(jnp.bfloat16)
    cs_pair = jnp.concatenate((cs_high, cs_low), axis=0)

    row = lax.broadcasted_iota(jnp.int32, (seqs, per_group * head_dim), 0)
    read = [jnp.zeros(row.shape, jnp.float32) for _ in range(groups)]
    for s in range(seqs):
        fetch_state[s].wait()
        for g in range(groups):
            span = slice(g * state_dim, (g + 1) * state_dim)
            fresh = []
            for h in range(g * per_group, (g + 1) * per_group):
                new = (
                    decay[s : s + 1, h : h + 1] * state[s, h]
                    + stepped[h * head_dim : (h + 1) * head_dim, s : s + 1] * bs[s : s + 1, span]
                )
                state[s, h] = new
                fresh.append(new.astype(jnp.bfloat16))
            both = lax.dot_general(
                cs_pair[:, span],
                jnp.concatenate(fresh, axis=0),
                (((1,), (1,)), ((), ())),
                preferred_element_type=jnp.float32,
            )
            read[g] = jnp.where(row == s, both[:seqs] + both[seqs:], read[g])
        if s > 0:
            put_state[s - 1].start()
    fetch[3].wait()
    gate = jax.nn.silu(project(wz[...]))
    put_state[seqs - 1].start()
    gated = (jnp.concatenate(read, axis=1) + wide[seqs:] * xs) * gate
    block = inner // groups
    for g in range(groups):
        span = slice(g * block, (g + 1) * block)
        part = gated[:, span]
        part = part * lax.rsqrt(jnp.mean(part * part, axis=-1, keepdims=True) + epsilon)
        mixed_ref[:, span] = (part * group_gain_ref[:, span]).astype(jnp.bfloat16)
    for copy in put_state:
        copy.wait()


def mixer(
    tokens,
    norm1_gain,
    ssm_state,
    conv_x,
    conv_b,
    conv_c,
    w_x,
    w_z,
    w_b,
    w_c,
    w_dt,
    dt_bias,
    a_log,
    d_skip,
    taps_x,
    taps_b,
    taps_c,
    group_gain,
):
    seqs = tokens.shape[0]
    vmem = pl.BlockSpec(memory_space=pltpu.VMEM)
    hbm = pl.BlockSpec(memory_space=pl.ANY)
    shape = jax.ShapeDtypeStruct
    taps_first = lambda a: a.transpose(1, 0, 2)
    conv_x, conv_b, conv_c = taps_first(conv_x), taps_first(conv_b), taps_first(conv_c)
    mixed, state, next_x, next_b, next_c = pl.pallas_call(
        mixer_kernel,
        out_shape=(
            shape((seqs, w_x.shape[1]), jnp.bfloat16),
            shape(ssm_state.shape, ssm_state.dtype),
            shape(conv_x.shape, conv_x.dtype),
            shape(conv_b.shape, conv_b.dtype),
            shape(conv_c.shape, conv_c.dtype),
        ),
        in_specs=[vmem, vmem, hbm, vmem, vmem, vmem, hbm, hbm, hbm, hbm] + [vmem] * 8,
        out_specs=(vmem, hbm, vmem, vmem, vmem),
        scratch_shapes=[
            pltpu.VMEM(w_x.shape, jnp.bfloat16),
            pltpu.VMEM(w_z.shape, jnp.bfloat16),
            pltpu.VMEM(w_b.shape, jnp.bfloat16),
            pltpu.VMEM(w_c.shape, jnp.bfloat16),
            pltpu.VMEM(ssm_state.shape, jnp.float32),
            pltpu.SemaphoreType.DMA((4,)),
            pltpu.SemaphoreType.DMA((seqs,)),
            pltpu.SemaphoreType.DMA((seqs,)),
        ],
        cost_estimate=pl.CostEstimate(flops=10**8, bytes_accessed=14 * 10**6, transcendentals=0),
    )(
        tokens,
        norm1_gain[None],
        ssm_state,
        conv_x,
        conv_b,
        conv_c,
        w_x,
        w_z,
        w_b,
        w_c,
        w_dt.T,
        dt_bias[None],
        a_log[None],
        d_skip[None],
        taps_x,
        taps_b,
        taps_c,
        group_gain[None],
    )
    return mixed, state, taps_first(next_x), taps_first(next_b), taps_first(next_c)


def tail_kernel(
    peers,
    splits,
    share,
    mixed_ref,
    w_out_hbm,
    tokens_ref,
    gain_ref,
    ids_ref,
    weights_ref,
    gate_hbm,
    up_hbm,
    down_hbm,
    dense_gate_ref,
    dense_up_ref,
    dense_down_ref,
    branch_ref,
    out_ref,
    w_out,
    gate_up,
    down,
    partials,
    features,
    tables,
    stage_ref,
    dense,
    packed,
    returned,
    load_sem,
    part_send,
    part_recv,
    feat_send,
    feat_recv,
    table_send,
    table_recv,
    dense_send,
    dense_recv,
    ret_send,
    ret_recv,
):
    ep = lax.axis_index("ep")
    tp = lax.axis_index("tp")
    everyone = peers * splits
    me = ep * splits + tp
    seqs, width = tokens_ref.shape
    hidden = down.shape[0]
    part = width // splits

    loads = [
        pltpu.make_async_copy(w_out_hbm, w_out, load_sem.at[0]),
        pltpu.make_async_copy(gate_hbm.at[0], gate_up.at[:, pl.ds(0, hidden)], load_sem.at[1]),
        pltpu.make_async_copy(up_hbm.at[0], gate_up.at[:, pl.ds(hidden, hidden)], load_sem.at[2]),
        pltpu.make_async_copy(down_hbm.at[0], down, load_sem.at[3]),
    ]
    for load in loads:
        load.start()

    barrier = pltpu.get_barrier_semaphore()

    def greet(i, carry):
        other = lax.rem(me + i, everyone)
        pl.semaphore_signal(
            barrier,
            inc=1,
            device_id={"ep": other // splits, "tp": lax.rem(other, splits)},
            device_id_type=pl.DeviceIdType.MESH,
        )
        return carry

    lax.fori_loop(1, everyone, greet, 0)

    lanes = lax.broadcasted_iota(jnp.int32, tables.shape[1:], 1)
    table = jnp.zeros(tables.shape[1:], jnp.float32)
    for k in range(ids_ref.shape[1]):
        table = table + jnp.where(lanes == ids_ref[:, k : k + 1], weights_ref[:, k : k + 1], 0.0)
    tables[ep] = table
    lane = lax.broadcasted_iota(jnp.int32, stage_ref.shape[1:], 1)
    for owner in range(peers):
        start = owner * share
        base = start // 128 * 128
        block = jnp.zeros(stage_ref.shape[1:], jnp.float32)
        for i, ref in enumerate((dense_gate_ref, dense_up_ref, dense_down_ref)):
            source = ref[:, base : base + 128].astype(jnp.float32)
            shift = (i * share - (start - base)) % 128
            if shift:
                source = pltpu.roll(source, shift, 1)
            block = jnp.where((lane >= i * share) & (lane < (i + 1) * share), source, block)
        stage_ref[owner] = block.astype(jnp.bfloat16)
    dense[ep] = stage_ref[ep]

    loads[0].wait()
    partial_out = jnp.dot(mixed_ref[...], w_out[...], preferred_element_type=jnp.float32)
    partials[tp] = partial_out.astype(jnp.bfloat16)

    pl.semaphore_wait(barrier, everyone - 1)

    def part_copy(i, slot):
        return pltpu.make_async_remote_copy(
            src_ref=partials.at[slot],
            dst_ref=partials.at[slot],
            send_sem=part_send.at[i],
            recv_sem=part_recv.at[slot],
            device_id={"ep": ep, "tp": lax.rem(tp + i, splits)},
            device_id_type=pl.DeviceIdType.MESH,
        )

    def table_copy(i, slot):
        return pltpu.make_async_remote_copy(
            src_ref=tables.at[slot],
            dst_ref=tables.at[slot],
            send_sem=table_send.at[i],
            recv_sem=table_recv.at[slot],
            device_id={"ep": lax.rem(ep + i, peers), "tp": tp},
            device_id_type=pl.DeviceIdType.MESH,
        )

    def dense_copy(i, slot):
        return pltpu.make_async_remote_copy(
            src_ref=stage_ref.at[lax.rem(ep + i, peers)],
            dst_ref=dense.at[slot],
            send_sem=dense_send.at[i],
            recv_sem=dense_recv.at[slot],
            device_id={"ep": lax.rem(ep + i, peers), "tp": tp},
            device_id_type=pl.DeviceIdType.MESH,
        )

    def feat_copy(i, slot):
        return pltpu.make_async_remote_copy(
            src_ref=features.at[slot],
            dst_ref=features.at[slot],
            send_sem=feat_send.at[i],
            recv_sem=feat_recv.at[slot],
            device_id={"ep": lax.rem(ep + i, peers), "tp": tp},
            device_id_type=pl.DeviceIdType.MESH,
        )

    def ret_copy(i, slot):
        other = lax.rem(me + i, everyone)
        return pltpu.make_async_remote_copy(
            src_ref=packed.at[lax.rem(other, splits), other // splits],
            dst_ref=returned.at[slot],
            send_sem=ret_send.at[i],
            recv_sem=ret_recv.at[slot],
            device_id={"ep": other // splits, "tp": lax.rem(other, splits)},
            device_id_type=pl.DeviceIdType.MESH,
        )

    def start_all(copy, slot, count):
        def step(i, carry):
            copy(i, slot).start()
            return carry

        lax.fori_loop(1, count, step, 0)

    def take_all(copy, own, count):
        def step(i, carry):
            copy(i, lax.rem(own + count - i, count)).wait_recv()
            return carry

        lax.fori_loop(1, count, step, 0)

    def sent_all(copy, slot, count):
        def step(i, carry):
            copy(i, slot).wait_send()
            return carry

        lax.fori_loop(1, count, step, 0)

    start_all(part_copy, tp, splits)
    start_all(table_copy, ep, peers)
    start_all(dense_copy, ep, peers)

    take_all(part_copy, tp, splits)
    summed = partials[0].astype(jnp.float32)
    for t in range(1, splits):
        summed = summed + partials[t].astype(jnp.float32)
    residual = (tokens_ref[...].astype(jnp.float32) + summed).astype(jnp.bfloat16)
    residual = residual.astype(jnp.float32)
    normed2 = rms_rows(residual, gain_ref[...]).astype(jnp.bfloat16)
    features[ep] = normed2
    start_all(feat_copy, ep, peers)

    take_all(table_copy, ep, peers)
    take_all(dense_copy, ep, peers)
    every_table = tables[...].reshape(peers * seqs, tables.shape[2])
    columns = lax.broadcasted_iota(jnp.int32, every_table.shape, 1)
    own_weight = jnp.sum(jnp.where(columns == ep, every_table, 0.0), axis=1, keepdims=True)
    dense_weights = dense[...].reshape(width, dense.shape[2])
    for load in loads[1:]:
        load.wait()

    take_all(feat_copy, ep, peers)
    rows = features[...].astype(jnp.float32).reshape(peers * seqs, width)
    rows16 = rows.astype(jnp.bfloat16)
    pre = jnp.dot(rows16, gate_up[...], preferred_element_type=jnp.float32)
    active = own_weight * (jax.nn.silu(pre[:, :hidden]) * pre[:, hidden:])
    dense_pre = jnp.dot(rows16, dense_weights, preferred_element_type=jnp.float32)
    branch = jax.nn.sigmoid(
        jnp.sum(rows * branch_ref[...].astype(jnp.float32), axis=1, keepdims=True)
    )
    lane = lax.broadcasted_iota(jnp.int32, dense_pre.shape, 1)
    dense_act = jax.nn.silu(pltpu.roll(dense_pre, 2 * share, 1)) * pltpu.roll(dense_pre, share, 1)
    dense_act = jnp.where((lane >= 2 * share) & (lane < 3 * share), branch * dense_act, 0.0)
    total = jnp.dot(active.astype(jnp.bfloat16), down[...], preferred_element_type=jnp.float32)
    total = total + lax.dot_general(
        dense_act.astype(jnp.bfloat16),
        dense_weights,
        (((1,), (1,)), ((), ())),
        preferred_element_type=jnp.float32,
    )
    for t in range(splits):
        packed[t] = (
            total[:, t * part : (t + 1) * part].reshape(peers, seqs, part).astype(jnp.bfloat16)
        )
    returned[me] = packed[tp, ep]
    start_all(ret_copy, me, everyone)

    sent_all(part_copy, tp, splits)
    sent_all(table_copy, ep, peers)
    sent_all(dense_copy, ep, peers)
    sent_all(feat_copy, ep, peers)
    own_rows = residual[:, :part]
    for t in range(1, splits):
        own_rows = jnp.where(tp == t, residual[:, t * part : (t + 1) * part], own_rows)

    take_all(ret_copy, me, everyone)
    mixed = own_rows + jnp.sum(returned[...].astype(jnp.float32), axis=0)
    out_ref[...] = mixed.astype(jnp.bfloat16)
    sent_all(ret_copy, me, everyone)


def after_mixer(
    mixed_heads,
    w_out,
    tokens,
    norm2_gain,
    route_ids,
    route_weights,
    exp_gate,
    exp_up,
    exp_down,
    dense_gate,
    dense_up,
    dense_down,
    branch_gate,
):
    peers = lax.axis_size("ep")
    splits = lax.axis_size("tp")
    seqs, width = tokens.shape
    depth, local_hidden = dense_gate.shape
    share = local_hidden // peers
    hidden = exp_gate.shape[2]
    part = width // splits
    lanes = -(-3 * share // 128) * 128
    vmem = pl.BlockSpec(memory_space=pltpu.VMEM)
    hbm = pl.BlockSpec(memory_space=pl.ANY)
    dma = lambda count: pltpu.SemaphoreType.DMA((count,))
    return pl.pallas_call(
        functools.partial(tail_kernel, peers, splits, share),
        out_shape=jax.ShapeDtypeStruct((seqs, part), jnp.bfloat16),
        in_specs=[vmem, hbm, vmem, vmem, vmem, vmem, hbm, hbm, hbm, vmem, vmem, vmem, vmem],
        out_specs=vmem,
        scratch_shapes=[
            pltpu.VMEM(w_out.shape, jnp.bfloat16),
            pltpu.VMEM((width, 2 * hidden), jnp.bfloat16),
            pltpu.VMEM((hidden, width), jnp.bfloat16),
            pltpu.VMEM((splits, seqs, width), jnp.bfloat16),
            pltpu.VMEM((peers, seqs, width), jnp.bfloat16),
            pltpu.VMEM((peers, seqs, 128), jnp.float32),
            pltpu.VMEM((peers, depth, lanes), jnp.bfloat16),
            pltpu.VMEM((peers, depth, lanes), jnp.bfloat16),
            pltpu.VMEM((splits, peers, seqs, part), jnp.bfloat16),
            pltpu.VMEM((peers * splits, seqs, part), jnp.bfloat16),
            dma(4),
            dma(splits),
            dma(splits),
            dma(peers),
            dma(peers),
            dma(peers),
            dma(peers),
            dma(peers),
            dma(peers),
            dma(peers * splits),
            dma(peers * splits),
        ],
        compiler_params=pltpu.CompilerParams(
            collective_id=0, has_side_effects=True
        ),
        cost_estimate=pl.CostEstimate(flops=10**9, bytes_accessed=10**7, transcendentals=0),
    )(
        mixed_heads,
        w_out,
        tokens,
        norm2_gain[None],
        route_ids,
        route_weights,
        exp_gate,
        exp_up,
        exp_down,
        dense_gate,
        dense_up,
        dense_down.T,
        branch_gate.astype(jnp.float32)[None],
    )


def body(
    tokens,
    ssm_state,
    conv_x,
    conv_b,
    conv_c,
    w_x,
    w_z,
    w_b,
    w_c,
    w_dt,
    dt_bias,
    a_log,
    d_skip,
    taps_x,
    taps_b,
    taps_c,
    norm1_gain,
    group_gain,
    w_out,
    norm2_gain,
    route_ids,
    route_weights,
    exp_gate,
    exp_up,
    exp_down,
    dense_gate,
    dense_up,
    dense_down,
    branch_gate,
):
    mixed_heads, state_next, conv_x_next, conv_b_next, conv_c_next = mixer(
        tokens,
        norm1_gain,
        ssm_state,
        conv_x,
        conv_b,
        conv_c,
        w_x,
        w_z,
        w_b,
        w_c,
        w_dt,
        dt_bias,
        a_log,
        d_skip,
        taps_x,
        taps_b,
        taps_c,
        group_gain,
    )
    mixed = after_mixer(
        mixed_heads,
        w_out,
        tokens,
        norm2_gain,
        route_ids,
        route_weights,
        exp_gate,
        exp_up,
        exp_down,
        dense_gate,
        dense_up,
        dense_down,
        branch_gate,
    )
    return (mixed, state_next, conv_x_next, conv_b_next, conv_c_next)


def solution(mesh):
    return jax.shard_map(
        body,
        mesh=mesh,
        in_specs=(
            P("ep", None),
            P("ep", "tp", None, None),
            P("ep", None, "tp"),
            P("ep", None, "tp"),
            P("ep", None, "tp"),
            P(None, "tp"),
            P(None, "tp"),
            P(None, "tp"),
            P(None, "tp"),
            P(),
            P("tp"),
            P("tp"),
            P("tp"),
            P(None, "tp"),
            P(None, "tp"),
            P(None, "tp"),
            P(),
            P("tp"),
            P("tp", None),
            P(),
            P("ep", None),
            P("ep", None),
            P("ep", None, "tp"),
            P("ep", None, "tp"),
            P("ep", "tp", None),
            P("ep", "tp"),
            P("ep", "tp"),
            P("tp", "ep"),
            P(),
        ),
        out_specs=(
            P("ep", "tp"),
            P("ep", "tp", None, None),
            P("ep", None, "tp"),
            P("ep", None, "tp"),
            P("ep", None, "tp"),
        ),
        check_vma=False,
    )
```

profile of v0, /device:TPU:0, one launch (start us, length us, event | category | flops | bytes accessed | tf_op | source)
XLA Modules:
  0.0 42.6 jit_solution(10092001844943056902)
XLA Ops:
  0.6 1.3 %broadcast_in_dim.31 = f32[1024]{0:T(1024)} convert(bf16[1024]{0:T(1024)(128)(2,1)} %param.57) | non-fusion elementwise | flops 1024 | bytes 6144 | tf_op jit(solution)/shard_map/broadcast_in_dim | solution.py:524
  1.9 8.9 %shard_map.308 = (bf16[8,1024]{1,0:T(8,128)(2,1)}, f32[8,16,64,128]{3,2,1,0:T(8,128)}, bf16[3,8,1024]{2,1,0:T(8,128)(2,1)}, bf16[3,8,512]{2,1,0:T(8,128)(2,1)}, bf16[3,8,512]{2,1,0:T(8,128)(2,1)}) custom-call(bf16[8,1024]{1,0:T(8,128)(2,1)} %tokens_ref.3, f32[1,1024]{1,0:T(1,128)} %bitcast.21, f32[8,16,64,128]{3,2,1,0:T(8,128)} %state_hbm.1, ...), custom_call_target="tpu_custom_call" | custom-call | flops 100000000 | bytes 14000000 | tf_op jit(solution)/shard_map/pallas_call | solution.py:177
  10.8 30.5 %shard_map.309 = bf16[8,512]{1,0:T(8,128)(2,1)} custom-call(bf16[8,1024]{1,0:T(8,128)(2,1)} %get-tuple-element.10.mixed_ref, bf16[1024,1024]{1,0:T(8,128)(2,1)} %w_out_hbm.1, bf16[8,1024]{1,0:T(8,128)(2,1)} %tokens_ref.3, f32[1,1024]{1,0:T(1,128)} %bitcast.23, s32[8,6]{1,0:T(8,128)} %ids_ref.1, f32[8,6]{1,0:T(8,128)} %weights_ref.1, ...), custom_call_target="tpu_custom_call" | custom-call | flops 1000000000 | bytes 10000000 | tf_op jit(solution)/shard_map/pallas_call | solution.py:479
  41.3 1.3 %copy.35 = bf16[8,512]{1,0:T(8,128)(2,1)} copy(bf16[8,512]{1,0:T(8,128)(2,1)} %shard_map.309) | data formatting | bytes 16384
where the time goes:
time: 42.9 us; the launch traced here: 42.6 us
  Pallas kernels  39.4 us (92%)
  local copies, waits for them, and re-layouts  1.3 us (3%)
  other arithmetic  1.28 us (3%)
  between operations  0.65 us (2%)
    pallas_call x1, Pallas kernels, after_mixer(): pl.pallas_call(functools.partial(tail_kernel, peers, splits, share), out_...  30.5 us
    pallas_call x1, Pallas kernels, mixer(): pl.pallas_call(mixer_kernel, out_shape=(shape((seqs, w_x.shape[1]), jnp.b...  8.92 us
    unnamed x1, local copies, waits for them, and re-layouts  1.3 us
    broadcast_in_dim x1, other arithmetic, after_mixer(): branch_gate.astype(jnp.float32)[None]  1.28 us

commit v1 on v0

v1 whole, which is shorter than its diff:
```python
import functools

import jax
import jax.numpy as jnp
from jax import lax
from jax.experimental import pallas as pl
from jax.experimental.pallas import tpu as pltpu
from jax.sharding import PartitionSpec as P

epsilon = 1e-06
cores = 2


def rms_rows(values, gain):
    return values * lax.rsqrt(jnp.mean(values * values, axis=-1, keepdims=True) + epsilon) * gain


def partner(index, i, count):
    if count & (count - 1):
        return lax.rem(index + i, count)
    bit = 1
    other = index
    while bit <= i:
        if i & bit:
            other = other + bit * (1 - 2 * lax.rem(lax.div(index, bit), 2))
        bit *= 2
    return other


def source(index, i, count):
    if count & (count - 1):
        return lax.rem(index + count - i, count)
    return partner(index, i, count)


def layer_kernel(
    peers,
    splits,
    share,
    tokens_ref,
    gain1_ref,
    prev_x_ref,
    prev_b_ref,
    prev_c_ref,
    wdt_ref,
    bias_ref,
    a_log_ref,
    skip_ref,
    taps_x_ref,
    taps_b_ref,
    taps_c_ref,
    group_gain_ref,
    gain2_ref,
    ids_ref,
    weights_ref,
    dense_gate_ref,
    dense_up_ref,
    dense_down_ref,
    branch_ref,
    state_hbm,
    wx_hbm,
    wz_hbm,
    wb_hbm,
    wc_hbm,
    w_out_hbm,
    gate_hbm,
    up_hbm,
    down_hbm,
    own_ref,
    returned,
    state,
    next_x_ref,
    next_b_ref,
    next_c_ref,
    wx,
    wz,
    wb,
    wc,
    w_out,
    gate_up,
    down,
    partials,
    features,
    tables,
    stage_ref,
    dense,
    half_out,
    half_in,
    packed,
    load_sem,
    in_sem,
    part_send,
    part_recv,
    feat_send,
    feat_recv,
    pair_send,
    pair_recv,
    half_send,
    half_recv,
    table_send,
    table_recv,
    dense_send,
    dense_recv,
    ret_send,
    ret_recv,
):
    ep = lax.axis_index("ep")
    tp = lax.axis_index("tp")
    everyone = peers * splits
    chips = peers // cores
    me = ep * splits + tp
    chip = ep // cores
    core = lax.rem(ep, cores)
    mate = 1 - core
    seqs, heads, head_dim, state_dim = state.shape
    width = tokens_ref.shape[1]
    groups = wb.shape[1] // state_dim
    per_group = heads // groups
    inner = heads * head_dim
    hidden = down.shape[0]
    part = width // splits

    loads = [
        pltpu.make_async_copy(hbm, vmem, load_sem.at[i])
        for i, (hbm, vmem) in enumerate(
            (
                (wx_hbm, wx),
                (wb_hbm, wb),
                (wc_hbm, wc),
                (wz_hbm, wz),
                (w_out_hbm, w_out),
                (gate_hbm.at[0], gate_up.at[:, pl.ds(0, hidden)]),
                (up_hbm.at[0], gate_up.at[:, pl.ds(hidden, hidden)]),
                (down_hbm.at[0], down),
            )
        )
    ]
    fetch_state = [
        pltpu.make_async_copy(state_hbm.at[s], state.at[s], in_sem.at[s]) for s in range(seqs)
    ]
    for copy in loads[:3] + fetch_state + loads[3:]:
        copy.start()

    barrier = pltpu.get_barrier_semaphore()

    def greet(i, carry):
        other = lax.rem(me + i, everyone)
        pl.semaphore_signal(
            barrier,
            inc=1,
            device_id={"ep": other // splits, "tp": lax.rem(other, splits)},
            device_id_type=pl.DeviceIdType.MESH,
        )
        return carry

    lax.fori_loop(1, everyone, greet, 0)

    def remote(src, dst, send, recv, to_ep, to_tp):
        return pltpu.make_async_remote_copy(
            src_ref=src,
            dst_ref=dst,
            send_sem=send,
            recv_sem=recv,
            device_id={"ep": to_ep, "tp": to_tp},
            device_id_type=pl.DeviceIdType.MESH,
        )

    def part_copy(i, slot):
        return remote(
            partials.at[slot],
            partials.at[slot],
            part_send.at[i],
            part_recv.at[slot],
            ep,
            partner(tp, i, splits),
        )

    def table_copy(i, slot):
        return remote(
            tables.at[lax.rem(slot, cores), slot // cores],
            tables.at[lax.rem(slot, cores), slot // cores],
            table_send.at[i],
            table_recv.at[slot],
            partner(ep, i, peers),
            tp,
        )

    def dense_copy(i, slot):
        other = partner(ep, i, peers)
        return remote(
            stage_ref.at[other], dense.at[slot], dense_send.at[i], dense_recv.at[slot], other, tp
        )

    def feat_copy(i, slot):
        block = features.at[core, slot]
        return remote(
            block,
            block,
            feat_send.at[i],
            feat_recv.at[slot],
            cores * partner(chip, i, chips) + core,
            tp,
        )

    def pair_copy(slot, of):
        block = features.at[of, slot]
        return remote(
            block, block, pair_send.at[slot], pair_recv.at[slot], cores * chip + mate, tp
        )

    half_copy = remote(
        half_out, half_in, half_send.at[0], half_recv.at[0], cores * chip + mate, tp
    )

    def ret_copy(i, j, slot):
        to_chip = partner(chip, i, chips)
        to_tp = partner(tp, j, splits)
        return remote(
            packed.at[to_tp, to_chip],
            returned.at[slot],
            ret_send.at[i * splits + j],
            ret_recv.at[slot],
            cores * to_chip + mate,
            to_tp,
        )

    def project(weights):
        out = jnp.dot(normed, weights, preferred_element_type=jnp.float32)
        return out.astype(jnp.bfloat16).astype(jnp.float32)

    def conv(prev_ref, fresh, taps_ref, next_ref):
        prev = prev_ref[...].astype(jnp.float32)
        taps = taps_ref[...].astype(jnp.float32)
        depth = prev.shape[0]
        summed = prev[0] * taps[0:1]
        for j in range(1, depth):
            summed = summed + prev[j] * taps[j : j + 1]
            next_ref[j - 1] = prev[j].astype(jnp.bfloat16)
        summed = summed + fresh * taps[depth : depth + 1]
        next_ref[depth - 1] = fresh.astype(jnp.bfloat16)
        return jax.nn.silu(summed)

    normed = rms_rows(tokens_ref[...].astype(jnp.float32), gain1_ref[...]).astype(jnp.bfloat16)
    all_dt = lax.dot_general(
        normed, wdt_ref[...], (((1,), (1,)), ((), ())), preferred_element_type=jnp.float32
    )
    dt_raw = all_dt[:, :heads]
    for t in range(1, all_dt.shape[1] // heads):
        dt_raw = jnp.where(tp == t, all_dt[:, t * heads : (t + 1) * heads], dt_raw)
    step = jax.nn.softplus(dt_raw + bias_ref[...])
    decay = jnp.exp(-step * jnp.exp(a_log_ref[...]))
    spread = lax.broadcasted_iota(jnp.int32, (heads, inner), 1) // head_dim
    spread = spread == lax.broadcasted_iota(jnp.int32, (heads, inner), 0)
    per_head = jnp.concatenate((step, jnp.broadcast_to(skip_ref[...], step.shape)), axis=0)
    wide = jnp.dot(
        per_head,
        spread.astype(jnp.float32),
        precision=lax.Precision.HIGHEST,
        preferred_element_type=jnp.float32,
    )

    lanes = lax.broadcasted_iota(jnp.int32, tables.shape[2:], 1)
    table = jnp.zeros(tables.shape[2:], jnp.float32)
    for k in range(ids_ref.shape[1]):
        table = table + jnp.where(lanes == ids_ref[:, k : k + 1], weights_ref[:, k : k + 1], 0.0)
    tables[core, chip] = table
    lane = lax.broadcasted_iota(jnp.int32, stage_ref.shape[1:], 1)
    for owner in range(peers):
        start = owner * share
        base = start // 128 * 128
        block = jnp.zeros(stage_ref.shape[1:], jnp.float32)
        for i, ref in enumerate((dense_gate_ref, dense_up_ref, dense_down_ref)):
            rows = ref[:, base : base + 128].astype(jnp.float32)
            shift = (i * share - (start - base)) % 128
            if shift:
                rows = pltpu.roll(rows, shift, 1)
            block = jnp.where((lane >= i * share) & (lane < (i + 1) * share), rows, block)
        stage_ref[owner] = block.astype(jnp.bfloat16)
    dense[ep] = stage_ref[ep]

    loads[0].wait()
    xs = conv(prev_x_ref, project(wx[...]), taps_x_ref, next_x_ref)
    pl.semaphore_wait(barrier, everyone - 1)
    for i in reversed(range(1, peers)):
        dense_copy(i, ep).start()
    for i in reversed(range(1, peers)):
        table_copy(i, ep).start()

    loads[1].wait()
    bs = conv(prev_b_ref, project(wb[...]), taps_b_ref, next_b_ref)
    loads[2].wait()
    cs = conv(prev_c_ref, project(wc[...]), taps_c_ref, next_c_ref)
    stepped = jnp.transpose(wide[:seqs] * xs)
    cs_high = cs.astype(jnp.bfloat16)
    cs_low = (cs - cs_high.astype(jnp.float32)).astype(jnp.bfloat16)
    cs_pair = jnp.concatenate((cs_high, cs_low), axis=0)

    row = lax.broadcasted_iota(jnp.int32, (seqs, per_group * head_dim), 0)
    read = [jnp.zeros(row.shape, jnp.float32) for _ in range(groups)]
    for s in range(seqs):
        fetch_state[s].wait()
        for g in range(groups):
            span = slice(g * state_dim, (g + 1) * state_dim)
            fresh = []
            for h in range(g * per_group, (g + 1) * per_group):
                new = (
                    decay[s : s + 1, h : h + 1] * state[s, h]
                    + stepped[h * head_dim : (h + 1) * head_dim, s : s + 1] * bs[s : s + 1, span]
                )
                state[s, h] = new
                fresh.append(new.astype(jnp.bfloat16))
            both = lax.dot_general(
                cs_pair[:, span],
                jnp.concatenate(fresh, axis=0),
                (((1,), (1,)), ((), ())),
                preferred_element_type=jnp.float32,
            )
            read[g] = jnp.where(row == s, both[:seqs] + both[seqs:], read[g])
    loads[3].wait()
    gate = jax.nn.silu(project(wz[...]))
    gated = (jnp.concatenate(read, axis=1) + wide[seqs:] * xs) * gate
    block = inner // groups
    mixed_heads = []
    for g in range(groups):
        span = slice(g * block, (g + 1) * block)
        piece = gated[:, span]
        piece = piece * lax.rsqrt(jnp.mean(piece * piece, axis=-1, keepdims=True) + epsilon)
        mixed_heads.append((piece * group_gain_ref[:, span]).astype(jnp.bfloat16))
    loads[4].wait()
    partial_out = jnp.dot(
        jnp.concatenate(mixed_heads, axis=1), w_out[...], preferred_element_type=jnp.float32
    )
    partials[tp] = partial_out.astype(jnp.bfloat16)
    for i in range(1, splits):
        part_copy(i, tp).start()

    for i in range(1, peers):
        table_copy(i, source(ep, i, peers)).wait_recv()
    for i in range(1, peers):
        dense_copy(i, source(ep, i, peers)).wait_recv()
    for load in loads[5:]:
        load.wait()

    for i in range(1, splits):
        part_copy(i, source(tp, i, splits)).wait_recv()
    summed = partials[0].astype(jnp.float32)
    for t in range(1, splits):
        summed = summed + partials[t].astype(jnp.float32)
    residual = (tokens_ref[...].astype(jnp.float32) + summed).astype(jnp.bfloat16)
    residual = residual.astype(jnp.float32)
    features[core, chip] = rms_rows(residual, gain2_ref[...]).astype(jnp.bfloat16)
    for i in reversed(range(1, chips)):
        feat_copy(i, chip).start()
    pair_copy(chip, core).start()

    own_rows = residual[:, :part]
    for t in range(1, splits):
        own_rows = jnp.where(tp == t, residual[:, t * part : (t + 1) * part], own_rows)
    own_ref[...] = own_rows

    for i in range(1, chips):
        slot = source(chip, i, chips)
        feat_copy(i, slot).wait_recv()
        pair_copy(slot, core).start()

    dense_weights = dense[...].reshape(width, dense.shape[2])
    rows_of = chips * seqs

    def feed_forward(of):
        rows16 = features[of].reshape(rows_of, width)
        weights = tables[of].reshape(rows_of, tables.shape[3])
        columns = lax.broadcasted_iota(jnp.int32, weights.shape, 1)
        weight = jnp.sum(jnp.where(columns == ep, weights, 0.0), axis=1, keepdims=True)
        pre = jnp.dot(rows16, gate_up[...], preferred_element_type=jnp.float32)
        active = weight * (jax.nn.silu(pre[:, :hidden]) * pre[:, hidden:])
        dense_pre = jnp.dot(rows16, dense_weights, preferred_element_type=jnp.float32)
        branch = jax.nn.sigmoid(
            jnp.sum(rows16.astype(jnp.float32) * branch_row, axis=1, keepdims=True)
        )
        lane = lax.broadcasted_iota(jnp.int32, dense_pre.shape, 1)
        dense_act = jax.nn.silu(pltpu.roll(dense_pre, 2 * share, 1))
        dense_act = dense_act * pltpu.roll(dense_pre, share, 1)
        dense_act = jnp.where((lane >= 2 * share) & (lane < 3 * share), branch * dense_act, 0.0)
        total = jnp.dot(active.astype(jnp.bfloat16), down[...], preferred_element_type=jnp.float32)
        return total + lax.dot_general(
            dense_act.astype(jnp.bfloat16),
            dense_weights,
            (((1,), (1,)), ((), ())),
            preferred_element_type=jnp.float32,
        )

    branch_row = branch_ref[...].astype(jnp.float32).reshape(1, width)
    half_out[...] = feed_forward(core).astype(jnp.bfloat16)
    half_copy.start()
    for i in range(chips):
        pair_copy(source(chip, i, chips) if i else chip, mate).wait_recv()
    total = feed_forward(mate)
    half_copy.wait_recv()
    total = total + half_in[...].astype(jnp.float32)
    for t in range(splits):
        packed[t] = (
            total[:, t * part : (t + 1) * part].reshape(chips, seqs, part).astype(jnp.bfloat16)
        )
    for i in reversed(range(chips)):
        for j in reversed(range(splits)):
            ret_copy(i, j, chip * splits + tp).start()

    for i in range(1, splits):
        part_copy(i, tp).wait_send()
    for i in range(1, peers):
        table_copy(i, ep).wait_send()
        dense_copy(i, ep).wait_send()
    for i in range(1, chips):
        feat_copy(i, chip).wait_send()
    for i in range(chips):
        pair_copy(source(chip, i, chips) if i else chip, core).wait_send()
    half_copy.wait_send()
    for i in range(chips):
        for j in range(splits):
            slot = (source(chip, i, chips) if i else chip) * splits
            slot = slot + (source(tp, j, splits) if j else tp)
            ret_copy(i, j, slot).wait_recv()
    for i in range(chips):
        for j in range(splits):
            ret_copy(i, j, chip * splits + tp).wait_send()


def finish_kernel(
    own_ref, returned, state, x_ref, b_ref, c_ref, out_ref, state_out, x_out, b_out, c_out, sum_ref, sem
):
    seqs = state.shape[0]
    puts = [pltpu.make_async_copy(state.at[s], state_out.at[s], sem.at[s]) for s in range(seqs)]
    for i, (ref, out) in enumerate(((x_ref, x_out), (b_ref, b_out), (c_ref, c_out))):
        puts.append(pltpu.make_async_copy(ref, out, sem.at[seqs + i]))
    for put in puts:
        put.start()
    mixed = own_ref[...] + jnp.sum(returned[...].astype(jnp.float32), axis=0)
    sum_ref[...] = mixed.astype(jnp.bfloat16)
    last = pltpu.make_async_copy(sum_ref, out_ref, sem.at[seqs + 3])
    last.start()
    for put in puts:
        put.wait()
    last.wait()


def body(
    tokens,
    ssm_state,
    conv_x,
    conv_b,
    conv_c,
    w_x,
    w_z,
    w_b,
    w_c,
    w_dt,
    dt_bias,
    a_log,
    d_skip,
    taps_x,
    taps_b,
    taps_c,
    norm1_gain,
    group_gain,
    w_out,
    norm2_gain,
    route_ids,
    route_weights,
    exp_gate,
    exp_up,
    exp_down,
    dense_gate,
    dense_up,
    dense_down,
    branch_gate,
):
    peers = lax.axis_size("ep")
    splits = lax.axis_size("tp")
    chips = peers // cores
    seqs, width = tokens.shape
    depth, local_hidden = dense_gate.shape
    share = local_hidden // peers
    hidden = exp_gate.shape[2]
    part = width // splits
    lanes = -(-3 * share // 128) * 128
    vmem = pl.BlockSpec(memory_space=pltpu.VMEM)
    hbm = pl.BlockSpec(memory_space=pltpu.HBM)
    dma = lambda count: pltpu.SemaphoreType.DMA((count,))
    taps_first = lambda a: a.transpose(1, 0, 2)
    conv_x, conv_b, conv_c = taps_first(conv_x), taps_first(conv_b), taps_first(conv_c)
    bf16, f32 = jnp.bfloat16, jnp.float32
    in_hbm = lambda a: pltpu.with_memory_space_constraint(a, pltpu.HBM)
    held = pl.pallas_call(
        functools.partial(layer_kernel, peers, splits, share),
        out_shape=(
            pltpu.VMEM((seqs, part), f32),
            pltpu.VMEM((chips * splits, seqs, part), bf16),
            pltpu.VMEM(ssm_state.shape, f32),
            pltpu.VMEM(conv_x.shape, bf16),
            pltpu.VMEM(conv_b.shape, bf16),
            pltpu.VMEM(conv_c.shape, bf16),
        ),
        in_specs=[vmem] * 20 + [hbm] * 9,
        out_specs=(vmem,) * 6,
        scratch_shapes=[
            pltpu.VMEM(w_x.shape, bf16),
            pltpu.VMEM(w_z.shape, bf16),
            pltpu.VMEM(w_b.shape, bf16),
            pltpu.VMEM(w_c.shape, bf16),
            pltpu.VMEM(w_out.shape, bf16),
            pltpu.VMEM((width, 2 * hidden), bf16),
            pltpu.VMEM((hidden, width), bf16),
            pltpu.VMEM((splits, seqs, width), bf16),
            pltpu.VMEM((cores, chips, seqs, width), bf16),
            pltpu.VMEM((cores, chips, seqs, 128), f32),
            pltpu.VMEM((peers, depth, lanes), bf16),
            pltpu.VMEM((peers, depth, lanes), bf16),
            pltpu.VMEM((chips * seqs, width), bf16),
            pltpu.VMEM((chips * seqs, width), bf16),
            pltpu.VMEM((splits, chips, seqs, part), bf16),
            dma(8),
            dma(seqs),
            dma(splits),
            dma(splits),
            dma(chips),
            dma(chips),
            dma(chips),
            dma(chips),
            dma(1),
            dma(1),
            dma(peers),
            dma(peers),
            dma(peers),
            dma(peers),
            dma(chips * splits),
            dma(chips * splits),
        ],
        compiler_params=pltpu.CompilerParams(
            collective_id=0, has_side_effects=True, vmem_limit_bytes=40 * 2**20
        ),
        cost_estimate=pl.CostEstimate(flops=10**9, bytes_accessed=2 * 10**7, transcendentals=0),
    )(*map(in_hbm, (
        tokens,
        norm1_gain[None],
        conv_x,
        conv_b,
        conv_c,
        w_dt.T,
        dt_bias[None],
        a_log[None],
        d_skip[None],
        taps_x,
        taps_b,
        taps_c,
        group_gain[None],
        norm2_gain[None],
        route_ids,
        route_weights,
        dense_gate,
        dense_up,
        dense_down.T,
        branch_gate,
        ssm_state,
        w_x,
        w_z,
        w_b,
        w_c,
        w_out,
        exp_gate,
        exp_up,
        exp_down,
    )))
    held = [pltpu.with_memory_space_constraint(a, pltpu.VMEM) for a in held]
    shape = jax.ShapeDtypeStruct
    mixed, state, next_x, next_b, next_c = pl.pallas_call(
        finish_kernel,
        out_shape=(
            shape((seqs, part), bf16),
            shape(ssm_state.shape, f32),
            shape(conv_x.shape, bf16),
            shape(conv_b.shape, bf16),
            shape(conv_c.shape, bf16),
        ),
        in_specs=[vmem] * 6,
        out_specs=(hbm,) * 5,
        scratch_shapes=[pltpu.VMEM((seqs, part), bf16), dma(seqs + 4)],
        compiler_params=pltpu.CompilerParams(vmem_limit_bytes=8 * 2**20),
        cost_estimate=pl.CostEstimate(flops=10**5, bytes_accessed=5 * 10**6, transcendentals=0),
    )(*held)
    return mixed, state, taps_first(next_x), taps_first(next_b), taps_first(next_c)


def solution(mesh):
    return jax.shard_map(
        body,
        mesh=mesh,
        in_specs=(
            P("ep", None),
            P("ep", "tp", None, None),
            P("ep", None, "tp"),
            P("ep", None, "tp"),
            P("ep", None, "tp"),
            P(None, "tp"),
            P(None, "tp"),
            P(None, "tp"),
            P(None, "tp"),
            P(),
            P("tp"),
            P("tp"),
            P("tp"),
            P(None, "tp"),
            P(None, "tp"),
            P(None, "tp"),
            P(),
            P("tp"),
            P("tp", None),
            P(),
            P("ep", None),
            P("ep", None),
            P("ep", None, "tp"),
            P("ep", None, "tp"),
            P("ep", "tp", None),
            P("ep", "tp"),
            P("ep", "tp"),
            P("tp", "ep"),
            P(),
        ),
        out_specs=(
            P("ep", "tp"),
            P("ep", "tp", None, None),
            P("ep", None, "tp"),
            P("ep", None, "tp"),
            P("ep", None, "tp"),
        ),
        check_vma=False,
    )
```

time: 42.9 us -> 33.5 us (0.78)
  Pallas kernels: 39.4 us -> 32.6 us
  local copies, waits for them, and re-layouts: 1.3 us -> 0 us
  other arithmetic: 1.28 us -> 0 us
    pallas_call x2, Pallas kernels: 39.4 us -> 32.6 us  [the longest x1 30.5 us: body(): pl.pallas_call(functools.partial(layer_kernel, peers, splits, share), out...]
    unnamed x1 -> x0, local copies, waits for them, and re-layouts: 1.3 us -> none
    broadcast_in_dim x1 -> x0, other arithmetic: 1.28 us -> none  [after_mixer(): branch_gate.astype(jnp.float32)[None]]
where the time goes in v1:
time: 33.5 us; the launch traced here: 33.3 us
  Pallas kernels  32.6 us (97%)
  between operations  0.65 us (2%)
    pallas_call x1, Pallas kernels, body(): pl.pallas_call(functools.partial(layer_kernel, peers, splits, share), out...  30.5 us
    pallas_call x1, Pallas kernels, body(): pl.pallas_call(finish_kernel, out_shape=(shape((seqs, part), bf16), shape...  2.12 us

profile of v1, /device:TPU:0, one launch (start us, length us, event | category | flops | bytes accessed | tf_op | source)
XLA Modules:
  0.0 33.3 jit_solution(4233989770264027742)
XLA Ops:
  0.6 30.5 %shard_map.308 = (f32[8,512]{1,0:T(8,128)S(1)}, bf16[16,8,512]{2,1,0:T(8,128)(2,1)S(1)}, f32[8,16,64,128]{3,2,1,0:T(8,128)S(1)}, bf16[3,8,1024]{2,1,0:T(8,128)(2...) custom-call(bf16[8,1024]{1,0:T(8,128)(2,1)} %tokens_ref.1, f32[1,1024]{1,0:T(1,128)} %bitcast.19, ...), custom_call_target="tpu_custom_call" | custom-call | flops 1000000000 | bytes 20000000 | tf_op jit(solution)/shard_map/pallas_call | solution.py:493
  31.2 2.1 %shard_map.309 = (bf16[8,512]{1,0:T(8,128)(2,1)}, f32[8,16,64,128]{3,2,1,0:T(8,128)}, bf16[3,8,1024]{2,1,0:T(8,128)(2,1)}, bf16[3,8,512]{2,1,0:T(8,128)(2,1)}, bf16[3,8,512]{2,1,0:T(8,128)(2,1)}) custom-call(f32[8,512]{1,0:T(8,128)S(1)} %get-tuple-element.16.own_ref, bf16[16,8,512]{2,1,0:T(8,128)(2,1)S(1)} %get-tuple-element.17.returned, ...), custom_call_target="tpu_custom_call" | custom-call | flops 100000 | bytes 5000000 | tf_op jit(solution)/shard_map/pallas_call | solution.py:575

commit v2 on v1

v2 whole, which is shorter than its diff:
```python
import functools

import jax
import jax.numpy as jnp
from jax import lax
from jax.experimental import pallas as pl
from jax.experimental.pallas import tpu as pltpu
from jax.sharding import PartitionSpec as P

epsilon = 1e-06
cores = 2


def rms_rows(values, gain):
    return values * lax.rsqrt(jnp.mean(values * values, axis=-1, keepdims=True) + epsilon) * gain


def partner(index, i, count):
    if count & (count - 1):
        return lax.rem(index + i, count)
    bit = 1
    other = index
    while bit <= i:
        if i & bit:
            other = other + bit * (1 - 2 * lax.rem(lax.div(index, bit), 2))
        bit *= 2
    return other


def source(index, i, count):
    if count & (count - 1):
        return lax.rem(index + count - i, count)
    return partner(index, i, count)


def layer_kernel(
    peers,
    splits,
    share,
    fold,
    tokens_hbm,
    gain1_hbm,
    prev_x_hbm,
    prev_b_hbm,
    prev_c_hbm,
    wdt_hbm,
    bias_hbm,
    a_log_hbm,
    skip_hbm,
    taps_x_hbm,
    taps_b_hbm,
    taps_c_hbm,
    group_gain_hbm,
    gain2_hbm,
    ids_hbm,
    weights_hbm,
    dense_gate_hbm,
    dense_up_hbm,
    dense_down_hbm,
    branch_hbm,
    state_hbm,
    wx_hbm,
    wz_hbm,
    wb_hbm,
    wc_hbm,
    w_out_hbm,
    gate_hbm,
    up_hbm,
    down_hbm,
    own_ref,
    returned,
    state,
    next_x_ref,
    next_b_ref,
    next_c_ref,
    tokens_ref,
    gain1_ref,
    wdt_ref,
    bias_ref,
    a_log_ref,
    skip_ref,
    prev_x_ref,
    prev_b_ref,
    prev_c_ref,
    taps_x_ref,
    taps_b_ref,
    taps_c_ref,
    group_gain_ref,
    gain2_ref,
    ids_ref,
    weights_ref,
    branch_ref,
    slabs,
    wx,
    wz,
    wb,
    wc,
    w_out,
    gate_up,
    down,
    decays,
    partials,
    features,
    stage_ref,
    arrived,
    dense,
    half_out,
    half_in,
    packed,
    small_sem,
    load_sem,
    in_sem,
    send_sem,
    part_recv,
    feat_recv,
    batch_recv,
):
    ep = lax.axis_index("ep")
    tp = lax.axis_index("tp")
    everyone = peers * splits
    chips = peers // cores
    me = ep * splits + tp
    chip = ep // cores
    core = lax.rem(ep, cores)
    mate = 1 - core
    seqs, heads, head_dim, state_dim = state.shape
    width = tokens_ref.shape[1]
    groups = wb.shape[1] // state_dim
    per_group = heads // groups
    inner = heads * head_dim
    hidden = down.shape[0]
    part = width // splits
    depth = slabs.shape[1]

    small = {
        name: pltpu.make_async_copy(hbm, vmem, small_sem.at[i])
        for i, (name, hbm, vmem) in enumerate(
            (
                ("tokens", tokens_hbm, tokens_ref),
                ("gain1", gain1_hbm, gain1_ref),
                ("wdt", wdt_hbm, wdt_ref),
                ("bias", bias_hbm, bias_ref),
                ("a_log", a_log_hbm, a_log_ref),
                ("skip", skip_hbm, skip_ref),
                ("prev_x", prev_x_hbm, prev_x_ref),
                ("taps_x", taps_x_hbm, taps_x_ref),
                ("prev_b", prev_b_hbm, prev_b_ref),
                ("taps_b", taps_b_hbm, taps_b_ref),
                ("prev_c", prev_c_hbm, prev_c_ref),
                ("taps_c", taps_c_hbm, taps_c_ref),
                ("group_gain", group_gain_hbm, group_gain_ref),
                ("gain2", gain2_hbm, gain2_ref),
                ("ids", ids_hbm, ids_ref),
                ("weights", weights_hbm, weights_ref),
                ("branch", branch_hbm, branch_ref),
            )
        )
    }

    def ready(*names):
        for name in names:
            small[name].wait()

    loads = [
        pltpu.make_async_copy(hbm, vmem, load_sem.at[i])
        for i, hbm, vmem in (
            (0, wx_hbm, wx),
            (1, wb_hbm, wb),
            (2, wc_hbm, wc),
            (3, wz_hbm, wz),
            (4, w_out_hbm, w_out),
            (5, gate_hbm.at[0], gate_up.at[:, pl.ds(0, hidden)]),
            (5, up_hbm.at[0], gate_up.at[:, pl.ds(hidden, hidden)]),
            (6, down_hbm.at[0], down),
            (7, dense_gate_hbm, slabs.at[0]),
            (7, dense_up_hbm, slabs.at[1]),
            (7, dense_down_hbm, slabs.at[2]),
        )
    ]
    fetch_state = [
        pltpu.make_async_copy(
            state_hbm.at[pl.ds(s, 2)], state.at[pl.ds(s, 2)], in_sem.at[s // 2]
        )
        for s in range(0, seqs, 2)
    ]
    for name in ("tokens", "gain1", "wdt", "bias", "a_log", "skip"):
        small[name].start()
    for copy in loads[8:] + loads[:1]:
        copy.start()
    for name in ("prev_x", "taps_x", "prev_b", "taps_b", "prev_c", "taps_c"):
        small[name].start()
    for copy in loads[1:3]:
        copy.start()
    for name in ("group_gain", "gain2", "ids", "weights", "branch"):
        small[name].start()

    barrier = pltpu.get_barrier_semaphore()

    def greet(to_ep, to_tp):
        pl.semaphore_signal(
            barrier,
            inc=1,
            device_id={"ep": to_ep, "tp": to_tp},
            device_id_type=pl.DeviceIdType.MESH,
        )

    for i in reversed(range(peers)):
        for j in range(splits):
            if i or j:
                greet(partner(ep, i, peers) if i else ep, partner(tp, j, splits) if j else tp)

    def remote(src, dst, send, recv, to_ep, to_tp):
        return pltpu.make_async_remote_copy(
            src_ref=src,
            dst_ref=dst,
            send_sem=send,
            recv_sem=recv,
            device_id={"ep": to_ep, "tp": to_tp},
            device_id_type=pl.DeviceIdType.MESH,
        )

    mate_ep = cores * chip + mate

    def part_copy(i, slot):
        return remote(
            partials.at[slot],
            partials.at[slot],
            send_sem.at[0],
            part_recv.at[slot],
            ep,
            partner(tp, i, splits),
        )

    def dense_copy(i):
        other = partner(ep, i, peers)
        return remote(
            stage_ref.at[other], arrived.at[ep], send_sem.at[1], batch_recv.at[0], other, tp
        )

    def feat_copy(i, slot):
        block = features.at[core, slot]
        return remote(
            block,
            block,
            send_sem.at[2],
            feat_recv.at[slot],
            cores * partner(chip, i, chips) + core,
            tp,
        )

    def pair_copy(slot):
        block = features.at[core, slot]
        return remote(block, block, send_sem.at[3], batch_recv.at[1], mate_ep, tp)

    half_copy = remote(half_out, half_in, send_sem.at[4], batch_recv.at[2], mate_ep, tp)

    def ret_copy(i, j):
        to_chip = partner(chip, i, chips) if i else chip
        to_tp = partner(tp, j, splits) if j else tp
        return remote(
            packed.at[to_tp, to_chip],
            returned.at[chip * splits + tp],
            send_sem.at[5],
            batch_recv.at[3],
            cores * to_chip + mate,
            to_tp,
        )

    def batch(ref, send, recv):
        return remote(ref, ref, send_sem.at[send], batch_recv.at[recv], mate_ep, tp)

    parts_out = remote(
        partials.at[pl.ds(0, splits - 1)],
        partials.at[pl.ds(0, splits - 1)],
        send_sem.at[0],
        part_recv.at[0],
        mate_ep,
        tp,
    )
    dense_all = batch(arrived.at[pl.ds(0, peers - 1)], 1, 0)
    feats_out = batch(features.at[0, pl.ds(0, chips - 1)], 2, 1)
    pairs_all = batch(features.at[mate], 3, 1)
    rets_all = batch(returned, 5, 3)

    def project(weights):
        out = jnp.dot(normed, weights, preferred_element_type=jnp.float32)
        return out.astype(jnp.bfloat16).astype(jnp.float32)

    def conv(prev_ref, fresh, taps_ref, next_ref):
        prev = prev_ref[...].astype(jnp.float32)
        taps = taps_ref[...].astype(jnp.float32)
        count = prev.shape[0]
        summed = prev[0] * taps[0:1]
        for j in range(1, count):
            summed = summed + prev[j] * taps[j : j + 1]
            next_ref[j - 1] = prev[j].astype(jnp.bfloat16)
        summed = summed + fresh * taps[count : count + 1]
        next_ref[count - 1] = fresh.astype(jnp.bfloat16)
        return jax.nn.silu(summed)

    high = lambda a: a.astype(jnp.bfloat16).astype(jnp.float32)
    late = 2 * ep >= peers

    def spread_dense():
        pl.semaphore_wait(barrier, everyone - 1)
        for i in reversed(range(1, peers)):
            dense_copy(i).start()

    ready("tokens", "gain1", "wdt", "bias", "a_log", "skip")
    for copy in fetch_state[: seqs // 4]:
        copy.start()
    normed = rms_rows(tokens_ref[...].astype(jnp.float32), gain1_ref[...]).astype(jnp.bfloat16)
    all_dt = lax.dot_general(
        normed, wdt_ref[...], (((1,), (1,)), ((), ())), preferred_element_type=jnp.float32
    )
    dt_raw = all_dt[:, :heads]
    for t in range(1, all_dt.shape[1] // heads):
        dt_raw = jnp.where(tp == t, all_dt[:, t * heads : (t + 1) * heads], dt_raw)
    step = jax.nn.softplus(dt_raw + bias_ref[...])
    decay = jnp.exp(-step * jnp.exp(a_log_ref[...]))
    for h in range(heads):
        decays[h] = jnp.broadcast_to(decay[:, h : h + 1], (seqs, state_dim))
    spread = lax.broadcasted_iota(jnp.int32, (heads, inner), 1) // head_dim
    spread = spread == lax.broadcasted_iota(jnp.int32, (heads, inner), 0)
    per_head = jnp.concatenate(
        (step, jnp.broadcast_to(skip_ref[...], step.shape), decay), axis=0
    )
    top = high(per_head)
    middle = high(per_head - top)
    pieces = jnp.concatenate((top, middle, per_head - top - middle), axis=0).astype(jnp.bfloat16)
    wide = jnp.dot(pieces, spread.astype(jnp.bfloat16), preferred_element_type=jnp.float32)
    wide = wide[: 3 * seqs] + wide[3 * seqs : 6 * seqs] + wide[6 * seqs :]

    for copy in fetch_state[seqs // 4 :]:
        copy.start()
    pltpu.make_async_copy(slabs, slabs, load_sem.at[7]).wait()
    rows = depth // fold
    lane = lax.broadcasted_iota(jnp.int32, (rows, stage_ref.shape[2]), 1)
    for owner in range(peers):
        start = owner * share
        base = start // 128 * 128
        block = []
        for a in range(3):
            found = jnp.zeros(lane.shape, jnp.float32)
            for q in range(fold):
                at = (q if fold > 1 else a) * share
                piece = slabs[a, q * rows : (q + 1) * rows, base : base + 128].astype(jnp.float32)
                shift = (at - (start - base)) % 128
                if shift:
                    piece = pltpu.roll(piece, shift, 1)
                found = jnp.where((lane >= at) & (lane < at + share), piece, found)
            block.append(found)
        if fold > 1:
            for a in range(3):
                stage_ref[owner, a * rows : (a + 1) * rows] = block[a].astype(jnp.bfloat16)
        else:
            stage_ref[owner] = (block[0] + block[1] + block[2]).astype(jnp.bfloat16)
    arrived[ep] = stage_ref[ep]

    loads[0].wait()
    ready("prev_x", "taps_x")
    xs = conv(prev_x_ref, project(wx[...]), taps_x_ref, next_x_ref)
    loads[3].start()
    pl.when(late)(spread_dense)
    loads[1].wait()
    ready("prev_b", "taps_b")
    bs = conv(prev_b_ref, project(wb[...]), taps_b_ref, next_b_ref)
    loads[2].wait()
    ready("prev_c", "taps_c")
    cs = conv(prev_c_ref, project(wc[...]), taps_c_ref, next_c_ref)
    stepped = wide[:seqs] * xs
    stepped_high = high(stepped)
    left = jnp.transpose(
        jnp.concatenate((stepped_high, stepped - stepped_high, stepped_high), axis=0)
    ).astype(jnp.bfloat16)
    bs_high = high(bs)
    right = jnp.concatenate((bs_high, bs_high, bs - bs_high), axis=0)
    cs_high = high(cs)
    turned = jnp.transpose(jnp.concatenate((cs_high, cs - cs_high), axis=0))
    turned_column = lax.rem(lax.broadcasted_iota(jnp.int32, (state_dim, 2 * seqs), 1), seqs)
    right_row = lax.rem(lax.broadcasted_iota(jnp.int32, (3 * seqs, state_dim), 0), seqs)
    block = per_group * head_dim
    read = [jnp.zeros((block, 2 * seqs), jnp.float32) for _ in range(groups)]
    for s0 in range(0, seqs, 2):
        pair = (s0, s0 + 1)
        if s0 == 2:
            loads[4].start()
        if s0 == seqs // 2:
            for copy in loads[5:8]:
                copy.start()
        fetch_state[s0 // 2].wait()
        for g in range(groups):
            span = slice(g * state_dim, (g + 1) * state_dim)
            old = [state[s, g * per_group : (g + 1) * per_group] for s in pair]
            readers = [jnp.where(turned_column == s, turned[span], 0.0) for s in pair]
            read[g] = read[g] + jnp.dot(
                jnp.concatenate(
                    [a.reshape(block, state_dim).astype(jnp.bfloat16) for a in old], axis=1
                ),
                jnp.concatenate(readers, axis=0).astype(jnp.bfloat16),
                preferred_element_type=jnp.float32,
            )
            adders = [jnp.where(right_row == s, right[:, span], 0.0) for s in pair]
            added = jnp.dot(
                left[g * block : (g + 1) * block],
                jnp.concatenate(adders, axis=1).astype(jnp.bfloat16),
                preferred_element_type=jnp.float32,
            )
            for k, s in enumerate(pair):
                for j in range(per_group):
                    h = g * per_group + j
                    state[s, h] = (
                        decays[h, s : s + 1] * old[k][j]
                        + added[
                            j * head_dim : (j + 1) * head_dim, k * state_dim : (k + 1) * state_dim
                        ]
                    )
    pl.when(jnp.logical_not(late))(spread_dense)
    turned = jnp.transpose(jnp.concatenate(read, axis=0))
    met = []
    for g in range(groups):
        span = slice(g * state_dim, (g + 1) * state_dim)
        dots = jnp.sum(bs[:, span] * cs[:, span], axis=1, keepdims=True)
        met.append(jnp.broadcast_to(dots, (seqs, block)))
    readout = wide[2 * seqs :] * (turned[:seqs] + turned[seqs:])
    readout = readout + stepped * jnp.concatenate(met, axis=1)
    loads[3].wait()
    gate = jax.nn.silu(project(wz[...]))
    gated = (readout + wide[seqs : 2 * seqs] * xs) * gate
    ready("group_gain", "gain2", "ids", "weights", "branch")
    block = inner // groups
    mixed_heads = []
    for g in range(groups):
        span = slice(g * block, (g + 1) * block)
        piece = gated[:, span]
        piece = piece * lax.rsqrt(jnp.mean(piece * piece, axis=-1, keepdims=True) + epsilon)
        mixed_heads.append((piece * group_gain_ref[:, span]).astype(jnp.bfloat16))
    loads[4].wait()
    partial_out = jnp.dot(
        jnp.concatenate(mixed_heads, axis=1), w_out[...], preferred_element_type=jnp.float32
    )
    partials[tp] = partial_out.astype(jnp.bfloat16)
    for i in range(1, splits):
        part_copy(i, tp).start()

    tail = features.shape[3] - width
    lanes = lax.broadcasted_iota(jnp.int32, (seqs, tail), 1)
    table = jnp.zeros((seqs, tail), jnp.float32)
    for k in range(ids_ref.shape[1]):
        table = table + jnp.where(
            lax.rem(lanes, peers) == ids_ref[:, k : k + 1], weights_ref[:, k : k + 1], 0.0
        )
    table = jnp.where(lanes < peers, high(table), table - high(table))
    features[core, chip, :, width:] = table.astype(jnp.bfloat16)

    for i in range(1, splits):
        part_copy(i, source(tp, i, splits)).wait_recv()
    summed = partials[0].astype(jnp.float32)
    for t in range(1, splits):
        summed = summed + partials[t].astype(jnp.float32)
    residual = (tokens_ref[...].astype(jnp.float32) + summed).astype(jnp.bfloat16)
    residual = residual.astype(jnp.float32)
    features[core, chip, :, :width] = rms_rows(residual, gain2_ref[...]).astype(jnp.bfloat16)
    for i in reversed(range(1, chips)):
        feat_copy(i, chip).start()
    pair_copy(chip).start()

    own_rows = residual[:, :part]
    for t in range(1, splits):
        own_rows = jnp.where(tp == t, residual[:, t * part : (t + 1) * part], own_rows)
    own_ref[...] = own_rows

    def collect(first, last):
        for i in range(first, last):
            slot = source(chip, i, chips)
            feat_copy(i, slot).wait_recv()
            pair_copy(slot).start()

    collect(1, chips // 2)
    dense_all.wait_recv()
    if fold > 1:
        for s in range(peers):
            for q in range(fold):
                found = jnp.zeros(lane.shape, jnp.float32)
                for a in range(3):
                    piece = arrived[s, a * rows : (a + 1) * rows].astype(jnp.float32)
                    shift = (a - q) * share % 128
                    if shift:
                        piece = pltpu.roll(piece, shift, 1)
                    found = jnp.where(
                        (lane >= a * share) & (lane < (a + 1) * share), piece, found
                    )
                at = s * depth + q * rows
                dense[at : at + rows] = found.astype(jnp.bfloat16)
        dense_weights = dense[...]
    else:
        dense_weights = arrived[...].reshape(width, arrived.shape[2])
    collect(chips // 2, chips)
    pltpu.make_async_copy(gate_up, gate_up, load_sem.at[5]).wait()
    loads[7].wait()
    rows_of = chips * seqs
    branch_row = branch_ref[...].astype(jnp.float32).reshape(1, width)

    def feed_forward(of):
        rows16 = features[of, :, :, :width].reshape(rows_of, width)
        weights = features[of, :, :, width:].reshape(rows_of, tail).astype(jnp.float32)
        columns = lax.broadcasted_iota(jnp.int32, weights.shape, 1)
        columns = (columns == ep) | (columns == ep + peers)
        weight = jnp.sum(jnp.where(columns, weights, 0.0), axis=1, keepdims=True)
        pre = jnp.dot(rows16, gate_up[...], preferred_element_type=jnp.float32)
        active = weight * (jax.nn.silu(pre[:, :hidden]) * pre[:, hidden:])
        dense_pre = jnp.dot(rows16, dense_weights, preferred_element_type=jnp.float32)
        branch = jax.nn.sigmoid(
            jnp.sum(rows16.astype(jnp.float32) * branch_row, axis=1, keepdims=True)
        )
        lane = lax.broadcasted_iota(jnp.int32, dense_pre.shape, 1)
        dense_act = jax.nn.silu(pltpu.roll(dense_pre, 2 * share, 1))
        dense_act = dense_act * pltpu.roll(dense_pre, share, 1)
        dense_act = jnp.where((lane >= 2 * share) & (lane < 3 * share), branch * dense_act, 0.0)
        total = jnp.dot(active.astype(jnp.bfloat16), down[...], preferred_element_type=jnp.float32)
        return total + lax.dot_general(
            dense_act.astype(jnp.bfloat16),
            dense_weights,
            (((1,), (1,)), ((), ())),
            preferred_element_type=jnp.float32,
        )

    half_out[...] = feed_forward(core).astype(jnp.bfloat16)
    half_copy.start()
    pairs_all.wait_recv()
    total = feed_forward(mate)
    half_copy.wait_recv()
    total = total + half_in[...].astype(jnp.float32)
    for t in range(splits):
        packed[t] = (
            total[:, t * part : (t + 1) * part].reshape(chips, seqs, part).astype(jnp.bfloat16)
        )
    for i in reversed(range(chips)):
        for j in reversed(range(splits)):
            ret_copy(i, j).start()

    parts_out.wait_send()
    dense_all.wait_send()
    feats_out.wait_send()
    pairs_all.wait_send()
    half_copy.wait_send()
    rets_all.wait_recv()
    rets_all.wait_send()


def finish_kernel(
    own_ref, returned, state, x_ref, b_ref, c_ref, out_ref, state_out, x_out, b_out, c_out, sum_ref, sem
):
    seqs = state.shape[0]
    for s in range(seqs):
        pltpu.make_async_copy(state.at[s], state_out.at[s], sem.at[0]).start()
    puts = [pltpu.make_async_copy(state, state_out, sem.at[0])]
    for i, (ref, out) in enumerate(((x_ref, x_out), (b_ref, b_out), (c_ref, c_out))):
        puts.append(pltpu.make_async_copy(ref, out, sem.at[1 + i]))
        puts[-1].start()
    mixed = own_ref[...] + jnp.sum(returned[...].astype(jnp.float32), axis=0)
    sum_ref[...] = mixed.astype(jnp.bfloat16)
    puts.append(pltpu.make_async_copy(sum_ref, out_ref, sem.at[4]))
    puts[-1].start()
    for put in puts:
        put.wait()


def body(
    tokens,
    ssm_state,
    conv_x,
    conv_b,
    conv_c,
    w_x,
    w_z,
    w_b,
    w_c,
    w_dt,
    dt_bias,
    a_log,
    d_skip,
    taps_x,
    taps_b,
    taps_c,
    norm1_gain,
    group_gain,
    w_out,
    norm2_gain,
    route_ids,
    route_weights,
    exp_gate,
    exp_up,
    exp_down,
    dense_gate,
    dense_up,
    dense_down,
    branch_gate,
):
    peers = lax.axis_size("ep")
    splits = lax.axis_size("tp")
    chips = peers // cores
    seqs, width = tokens.shape
    depth, local_hidden = dense_gate.shape
    share = local_hidden // peers
    hidden = exp_gate.shape[2]
    part = width // splits
    heads, state_dim = ssm_state.shape[1], ssm_state.shape[3]
    fold = 128 // share
    if share * fold != 128 or depth % (16 * fold):
        fold = 1
    slab = (peers, 3 * depth // fold if fold > 1 else depth, 128)
    tail = -(-2 * peers // 128) * 128
    vmem = pl.BlockSpec(memory_space=pltpu.VMEM)
    hbm = pl.BlockSpec(memory_space=pltpu.HBM)
    dma = lambda count: pltpu.SemaphoreType.DMA((count,))
    taps_first = lambda a: a.transpose(1, 0, 2)
    conv_x, conv_b, conv_c = taps_first(conv_x), taps_first(conv_b), taps_first(conv_c)
    bf16, f32 = jnp.bfloat16, jnp.float32
    in_hbm = lambda a: pltpu.with_memory_space_constraint(a, pltpu.HBM)
    held = pl.pallas_call(
        functools.partial(layer_kernel, peers, splits, share, fold),
        out_shape=(
            pltpu.VMEM((seqs, part), f32),
            pltpu.VMEM((chips * splits, seqs, part), bf16),
            pltpu.VMEM(ssm_state.shape, f32),
            pltpu.VMEM(conv_x.shape, bf16),
            pltpu.VMEM(conv_b.shape, bf16),
            pltpu.VMEM(conv_c.shape, bf16),
        ),
        in_specs=[hbm] * 29,
        out_specs=(vmem,) * 6,
        scratch_shapes=[
            pltpu.VMEM(tokens.shape, bf16),
            pltpu.VMEM((1, width), f32),
            pltpu.VMEM(w_dt.shape[::-1], bf16),
            pltpu.VMEM((1, heads), f32),
            pltpu.VMEM((1, heads), f32),
            pltpu.VMEM((1, heads), f32),
            pltpu.VMEM(conv_x.shape, bf16),
            pltpu.VMEM(conv_b.shape, bf16),
            pltpu.VMEM(conv_c.shape, bf16),
            pltpu.VMEM(taps_x.shape, bf16),
            pltpu.VMEM(taps_b.shape, bf16),
            pltpu.VMEM(taps_c.shape, bf16),
            pltpu.VMEM((1, w_x.shape[1]), f32),
            pltpu.VMEM((1, width), f32),
            pltpu.VMEM(route_ids.shape, jnp.int32),
            pltpu.VMEM(route_weights.shape, f32),
            pltpu.VMEM((width,), bf16),
            pltpu.VMEM((3, depth, local_hidden), bf16),
            pltpu.VMEM(w_x.shape, bf16),
            pltpu.VMEM(w_z.shape, bf16),
            pltpu.VMEM(w_b.shape, bf16),
            pltpu.VMEM(w_c.shape, bf16),
            pltpu.VMEM(w_out.shape, bf16),
            pltpu.VMEM((width, 2 * hidden), bf16),
            pltpu.VMEM((hidden, width), bf16),
            pltpu.VMEM((heads, seqs, state_dim), f32),
            pltpu.VMEM((splits, seqs, width), bf16),
            pltpu.VMEM((cores, chips, seqs, width + tail), bf16),
            pltpu.VMEM(slab, bf16),
            pltpu.VMEM(slab, bf16),
            pltpu.VMEM((width, 128), bf16),
            pltpu.VMEM((chips * seqs, width), bf16),
            pltpu.VMEM((chips * seqs, width), bf16),
            pltpu.VMEM((splits, chips, seqs, part), bf16),
            dma(17),
            dma(8),
            dma(seqs // 2),
            dma(6),
            dma(splits),
            dma(chips),
            dma(4),
        ],
        compiler_params=pltpu.CompilerParams(
            collective_id=0, has_side_effects=True, vmem_limit_bytes=40 * 2**20
        ),
        cost_estimate=pl.CostEstimate(flops=10**9, bytes_accessed=2 * 10**7, transcendentals=0),
    )(*map(in_hbm, (
        tokens,
        norm1_gain[None],
        conv_x,
        conv_b,
        conv_c,
        w_dt.T,
        dt_bias[None],
        a_log[None],
        d_skip[None],
        taps_x,
        taps_b,
        taps_c,
        group_gain[None],
        norm2_gain[None],
        route_ids,
        route_weights,
        dense_gate,
        dense_up,
        dense_down.T,
        branch_gate,
        ssm_state,
        w_x,
        w_z,
        w_b,
        w_c,
        w_out,
        exp_gate,
        exp_up,
        exp_down,
    )))
    held = [pltpu.with_memory_space_constraint(a, pltpu.VMEM) for a in held]
    shape = jax.ShapeDtypeStruct
    mixed, state, next_x, next_b, next_c = pl.pallas_call(
        finish_kernel,
        out_shape=(
            shape((seqs, part), bf16),
            shape(ssm_state.shape, f32),
            shape(conv_x.shape, bf16),
            shape(conv_b.shape, bf16),
            shape(conv_c.shape, bf16),
        ),
        in_specs=[vmem] * 6,
        out_specs=(hbm,) * 5,
        scratch_shapes=[pltpu.VMEM((seqs, part), bf16), dma(5)],
        compiler_params=pltpu.CompilerParams(vmem_limit_bytes=8 * 2**20),
        cost_estimate=pl.CostEstimate(flops=10**5, bytes_accessed=5 * 10**6, transcendentals=0),
    )(*held)
    return mixed, state, taps_first(next_x), taps_first(next_b), taps_first(next_c)


def solution(mesh):
    return jax.shard_map(
        body,
        mesh=mesh,
        in_specs=(
            P("ep", None),
            P("ep", "tp", None, None),
            P("ep", None, "tp"),
            P("ep", None, "tp"),
            P("ep", None, "tp"),
            P(None, "tp"),
            P(None, "tp"),
            P(None, "tp"),
            P(None, "tp"),
            P(),
            P("tp"),
            P("tp"),
            P("tp"),
            P(None, "tp"),
            P(None, "tp"),
            P(None, "tp"),
            P(),
            P("tp"),
            P("tp", None),
            P(),
            P("ep", None),
            P("ep", None),
            P("ep", None, "tp"),
            P("ep", None, "tp"),
            P("ep", "tp", None),
            P("ep", "tp"),
            P("ep", "tp"),
            P("tp", "ep"),
            P(),
        ),
        out_specs=(
            P("ep", "tp"),
            P("ep", "tp", None, None),
            P("ep", None, "tp"),
            P("ep", None, "tp"),
            P("ep", None, "tp"),
        ),
        check_vma=False,
    )
```

time: 33.5 us -> 27.6 us (0.82)
  Pallas kernels: 32.6 us -> 26.7 us
    pallas_call x1, Pallas kernels: 30.5 us -> 24.7 us  [body(): pl.pallas_call(functools.partial(layer_kernel, peers, splits, share, fold...]
where the time goes in v2:
time: 27.6 us; the launch traced here: 27.4 us
  Pallas kernels  26.7 us (97%)
  between operations  0.65 us (2%)
    pallas_call x1, Pallas kernels, body(): pl.pallas_call(functools.partial(layer_kernel, peers, splits, share, fold...  24.7 us
    pallas_call x1, Pallas kernels, body(): pl.pallas_call(finish_kernel, out_shape=(shape((seqs, part), bf16), shape...  2.06 us

profile of v2, /device:TPU:0, one launch (start us, length us, event | category | flops | bytes accessed | tf_op | source)
XLA Modules:
  0.0 27.4 jit_solution(2412667524588637792)
XLA Ops:
  0.6 24.7 %shard_map.308 = (f32[8,512]{1,0:T(8,128)S(1)}, bf16[16,8,512]{2,1,0:T(8,128)(2,1)S(1)}, f32[8,16,64,128]{3,2,1,0:T(8,128)S(1)}, bf16[3,8,1024]{2,1,0:T(8,128)(2...) custom-call(bf16[8,1024]{1,0:T(8,128)(2,1)} %tokens_hbm.1, f32[1,1024]{1,0:T(1,128)} %bitcast.19, ...), custom_call_target="tpu_custom_call" | custom-call | flops 1000000000 | bytes 20000000 | tf_op jit(solution)/shard_map/pallas_call | solution.py:621
  25.3 2.1 %shard_map.309 = (bf16[8,512]{1,0:T(8,128)(2,1)}, f32[8,16,64,128]{3,2,1,0:T(8,128)}, bf16[3,8,1024]{2,1,0:T(8,128)(2,1)}, bf16[3,8,512]{2,1,0:T(8,128)(2,1)}, bf16[3,8,512]{2,1,0:T(8,128)(2,1)}) custom-call(f32[8,512]{1,0:T(8,128)S(1)} %get-tuple-element.16.own_ref, bf16[16,8,512]{2,1,0:T(8,128)(2,1)S(1)} %get-tuple-element.17.returned, ...), custom_call_target="tpu_custom_call" | custom-call | flops 100000 | bytes 5000000 | tf_op jit(solution)/shard_map/pallas_call | solution.py:713

commit v3 on v2

--- a/solution.py
+++ b/solution.py
@@ -122,7 +122,6 @@
     me = ep * splits + tp
     chip = ep // cores
     core = lax.rem(ep, cores)
-    mate = 1 - core
     seqs, heads, head_dim, state_dim = state.shape
     width = tokens_ref.shape[1]
     groups = wb.shape[1] // state_dim
@@ -161,22 +160,37 @@
         for name in names:
             small[name].wait()
 
-    loads = [
+    def in_pieces(hbm, vmem, sem, pieces):
+        step = vmem.shape[0] // pieces
+        return [
+            pltpu.make_async_copy(
+                hbm.at[pl.ds(i * step, step)], vmem.at[pl.ds(i * step, step)], sem
+            )
+            for i in range(pieces)
+        ]
+
+    wholes = (
+        (wx_hbm, wx, 8),
+        (wb_hbm, wb, 4),
+        (wc_hbm, wc, 4),
+        (wz_hbm, wz, 8),
+        (w_out_hbm, w_out, 8),
+    )
+    chunks_of = [in_pieces(a, b, load_sem.at[i], n) for i, (a, b, n) in enumerate(wholes)]
+    loaded = [pltpu.make_async_copy(b, b, load_sem.at[i]) for i, (_, b, _) in enumerate(wholes)]
+    expert_loads = [
         pltpu.make_async_copy(hbm, vmem, load_sem.at[i])
         for i, hbm, vmem in (
-            (0, wx_hbm, wx),
-            (1, wb_hbm, wb),
-            (2, wc_hbm, wc),
-            (3, wz_hbm, wz),
-            (4, w_out_hbm, w_out),
             (5, gate_hbm.at[0], gate_up.at[:, pl.ds(0, hidden)]),
             (5, up_hbm.at[0], gate_up.at[:, pl.ds(hidden, hidden)]),
             (6, down_hbm.at[0], down),
-            (7, dense_gate_hbm, slabs.at[0]),
-            (7, dense_up_hbm, slabs.at[1]),
-            (7, dense_down_hbm, slabs.at[2]),
         )
     ]
+    slab_loads = [
+        pltpu.make_async_copy(hbm, slabs.at[i], load_sem.at[7])
+        for i, hbm in enumerate((dense_gate_hbm, dense_up_hbm, dense_down_hbm))
+    ]
+
     fetch_state = [
         pltpu.make_async_copy(
             state_hbm.at[pl.ds(s, 2)], state.at[pl.ds(s, 2)], in_sem.at[s // 2]
@@ -185,13 +199,9 @@
     ]
     for name in ("tokens", "gain1", "wdt", "bias", "a_log", "skip"):
         small[name].start()
-    for copy in loads[8:] + loads[:1]:
+    for copy in slab_loads + chunks_of[0]:
         copy.start()
     for name in ("prev_x", "taps_x", "prev_b", "taps_b", "prev_c", "taps_c"):
-        small[name].start()
-    for copy in loads[1:3]:
-        copy.start()
-    for name in ("group_gain", "gain2", "ids", "weights", "branch"):
         small[name].start()
 
     barrier = pltpu.get_barrier_semaphore()
@@ -208,6 +218,11 @@
         for j in range(splits):
             if i or j:
                 greet(partner(ep, i, peers) if i else ep, partner(tp, j, splits) if j else tp)
+
+    for copy in chunks_of[1] + chunks_of[2]:
+        copy.start()
+    for name in ("group_gain", "gain2", "ids", "weights", "branch"):
+        small[name].start()
 
     def remote(src, dst, send, recv, to_ep, to_tp):
         return pltpu.make_async_remote_copy(
@@ -219,7 +234,7 @@
             device_id_type=pl.DeviceIdType.MESH,
         )
 
-    mate_ep = cores * chip + mate
+    mate_ep = cores * chip + 1 - core
 
     def part_copy(i, slot):
         return remote(
@@ -237,22 +252,22 @@
             stage_ref.at[other], arrived.at[ep], send_sem.at[1], batch_recv.at[0], other, tp
         )
 
-    def feat_copy(i, slot):
-        block = features.at[core, slot]
+    def feat_copy(i, of, slot):
+        block = features.at[of, slot]
         return remote(
             block,
             block,
             send_sem.at[2],
-            feat_recv.at[slot],
-            cores * partner(chip, i, chips) + core,
+            feat_recv.at[of, slot],
+            cores * partner(chip, i, chips) + 1,
             tp,
         )
 
-    def pair_copy(slot):
-        block = features.at[core, slot]
-        return remote(block, block, send_sem.at[3], batch_recv.at[1], mate_ep, tp)
-
-    half_copy = remote(half_out, half_in, send_sem.at[4], batch_recv.at[2], mate_ep, tp)
+    def pair_copy(of, slot):
+        block = features.at[of, slot]
+        return remote(block, block, send_sem.at[3], batch_recv.at[1 + of], mate_ep, tp)
+
+    half_copy = remote(half_out, half_in, send_sem.at[4], batch_recv.at[3], mate_ep, tp)
 
     def ret_copy(i, j):
         to_chip = partner(chip, i, chips) if i else chip
@@ -261,8 +276,8 @@
             packed.at[to_tp, to_chip],
             returned.at[chip * splits + tp],
             send_sem.at[5],
-            batch_recv.at[3],
-            cores * to_chip + mate,
+            batch_recv.at[4],
+            cores * to_chip + core,
             to_tp,
         )
 
@@ -278,9 +293,8 @@
         tp,
     )
     dense_all = batch(arrived.at[pl.ds(0, peers - 1)], 1, 0)
-    feats_out = batch(features.at[0, pl.ds(0, chips - 1)], 2, 1)
-    pairs_all = batch(features.at[mate], 3, 1)
-    rets_all = batch(returned, 5, 3)
+    others = pl.ds(0, chips - 1)
+    rets_all = batch(returned.at[pl.ds(0, chips * splits - 1)], 5, 4)
 
     def project(weights):
         out = jnp.dot(normed, weights, preferred_element_type=jnp.float32)
@@ -299,16 +313,22 @@
         return jax.nn.silu(summed)
 
     high = lambda a: a.astype(jnp.bfloat16).astype(jnp.float32)
-    late = 2 * ep >= peers
-
-    def spread_dense():
-        pl.semaphore_wait(barrier, everyone - 1)
+    quarter = 4 * ep // peers
+
+    def send_dense():
         for i in reversed(range(1, peers)):
             dense_copy(i).start()
 
+    def meet_and_send(at):
+        @pl.when(quarter == at)
+        def _():
+            pl.semaphore_wait(barrier, everyone - 1)
+            send_dense()
+
     ready("tokens", "gain1", "wdt", "bias", "a_log", "skip")
-    for copy in fetch_state[: seqs // 4]:
+    for copy in fetch_state:
         copy.start()
+    pltpu.make_async_copy(slabs, slabs, load_sem.at[7]).wait()
     normed = rms_rows(tokens_ref[...].astype(jnp.float32), gain1_ref[...]).astype(jnp.bfloat16)
     all_dt = lax.dot_general(
         normed, wdt_ref[...], (((1,), (1,)), ((), ())), preferred_element_type=jnp.float32
@@ -331,9 +351,6 @@
     wide = jnp.dot(pieces, spread.astype(jnp.bfloat16), preferred_element_type=jnp.float32)
     wide = wide[: 3 * seqs] + wide[3 * seqs : 6 * seqs] + wide[6 * seqs :]
 
-    for copy in fetch_state[seqs // 4 :]:
-        copy.start()
-    pltpu.make_async_copy(slabs, slabs, load_sem.at[7]).wait()
     rows = depth // fold
     lane = lax.broadcasted_iota(jnp.int32, (rows, stage_ref.shape[2]), 1)
     for owner in range(peers):
@@ -357,15 +374,16 @@
             stage_ref[owner] = (block[0] + block[1] + block[2]).astype(jnp.bfloat16)
     arrived[ep] = stage_ref[ep]
 
-    loads[0].wait()
+    loaded[0].wait()
     ready("prev_x", "taps_x")
     xs = conv(prev_x_ref, project(wx[...]), taps_x_ref, next_x_ref)
-    loads[3].start()
-    pl.when(late)(spread_dense)
-    loads[1].wait()
+    for copy in chunks_of[3]:
+        copy.start()
+    meet_and_send(3)
+    loaded[1].wait()
     ready("prev_b", "taps_b")
     bs = conv(prev_b_ref, project(wb[...]), taps_b_ref, next_b_ref)
-    loads[2].wait()
+    loaded[2].wait()
     ready("prev_c", "taps_c")
     cs = conv(prev_c_ref, project(wc[...]), taps_c_ref, next_c_ref)
     stepped = wide[:seqs] * xs
@@ -376,30 +394,35 @@
     bs_high = high(bs)
     right = jnp.concatenate((bs_high, bs_high, bs - bs_high), axis=0)
     cs_high = high(cs)
-    turned = jnp.transpose(jnp.concatenate((cs_high, cs - cs_high), axis=0))
-    turned_column = lax.rem(lax.broadcasted_iota(jnp.int32, (state_dim, 2 * seqs), 1), seqs)
+    cs_pair = jnp.concatenate((cs_high, cs - cs_high), axis=0).astype(jnp.bfloat16)
     right_row = lax.rem(lax.broadcasted_iota(jnp.int32, (3 * seqs, state_dim), 0), seqs)
     block = per_group * head_dim
-    read = [jnp.zeros((block, 2 * seqs), jnp.float32) for _ in range(groups)]
+    row = lax.broadcasted_iota(jnp.int32, (seqs, block), 0)
+    read = [jnp.zeros((seqs, block), jnp.float32) for _ in range(groups)]
     for s0 in range(0, seqs, 2):
         pair = (s0, s0 + 1)
         if s0 == 2:
-            loads[4].start()
+            for copy in chunks_of[4]:
+                copy.start()
         if s0 == seqs // 2:
-            for copy in loads[5:8]:
+            for copy in expert_loads:
                 copy.start()
+        if s0 == 0:
+            meet_and_send(2)
+        if s0 == seqs // 2:
+            meet_and_send(1)
         fetch_state[s0 // 2].wait()
         for g in range(groups):
             span = slice(g * state_dim, (g + 1) * state_dim)
             old = [state[s, g * per_group : (g + 1) * per_group] for s in pair]
-            readers = [jnp.where(turned_column == s, turned[span], 0.0) for s in pair]
-            read[g] = read[g] + jnp.dot(
-                jnp.concatenate(
-                    [a.reshape(block, state_dim).astype(jnp.bfloat16) for a in old], axis=1
-                ),
-                jnp.concatenate(readers, axis=0).astype(jnp.bfloat16),
-                preferred_element_type=jnp.float32,
-            )
+            for k, s in enumerate(pair):
+                both = lax.dot_general(
+                    cs_pair[:, span],
+                    old[k].reshape(block, state_dim).astype(jnp.bfloat16),
+                    (((1,), (1,)), ((), ())),
+                    preferred_element_type=jnp.float32,
+                )
+                read[g] = jnp.where(row == s, both[:seqs] + both[seqs:], read[g])
             adders = [jnp.where(right_row == s, right[:, span], 0.0) for s in pair]
             added = jnp.dot(
                 left[g * block : (g + 1) * block],
@@ -415,16 +438,14 @@
                             j * head_dim : (j + 1) * head_dim, k * state_dim : (k + 1) * state_dim
                         ]
                     )
-    pl.when(jnp.logical_not(late))(spread_dense)
-    turned = jnp.transpose(jnp.concatenate(read, axis=0))
     met = []
     for g in range(groups):
         span = slice(g * state_dim, (g + 1) * state_dim)
         dots = jnp.sum(bs[:, span] * cs[:, span], axis=1, keepdims=True)
         met.append(jnp.broadcast_to(dots, (seqs, block)))
-    readout = wide[2 * seqs :] * (turned[:seqs] + turned[seqs:])
+    readout = wide[2 * seqs :] * jnp.concatenate(read, axis=1)
     readout = readout + stepped * jnp.concatenate(met, axis=1)
-    loads[3].wait()
+    loaded[3].wait()
     gate = jax.nn.silu(project(wz[...]))
     gated = (readout + wide[seqs : 2 * seqs] * xs) * gate
     ready("group_gain", "gain2", "ids", "weights", "branch")
@@ -435,13 +456,19 @@
         piece = gated[:, span]
         piece = piece * lax.rsqrt(jnp.mean(piece * piece, axis=-1, keepdims=True) + epsilon)
         mixed_heads.append((piece * group_gain_ref[:, span]).astype(jnp.bfloat16))
-    loads[4].wait()
+    loaded[4].wait()
     partial_out = jnp.dot(
         jnp.concatenate(mixed_heads, axis=1), w_out[...], preferred_element_type=jnp.float32
     )
     partials[tp] = partial_out.astype(jnp.bfloat16)
+
+    @pl.when(quarter == 0)
+    def _():
+        pl.semaphore_wait(barrier, everyone - 1)
+
     for i in range(1, splits):
         part_copy(i, tp).start()
+    pl.when(quarter == 0)(send_dense)
 
     tail = features.shape[3] - width
     lanes = lax.broadcasted_iota(jnp.int32, (seqs, tail), 1)
@@ -462,21 +489,38 @@
     residual = residual.astype(jnp.float32)
     features[core, chip, :, :width] = rms_rows(residual, gain2_ref[...]).astype(jnp.bfloat16)
     for i in reversed(range(1, chips)):
-        feat_copy(i, chip).start()
-    pair_copy(chip).start()
+        feat_copy(i, core, chip).start()
+
+    @pl.when(core == 0)
+    def _():
+        remote(
+            features.at[0, chip],
+            features.at[0, chip],
+            send_sem.at[2],
+            feat_recv.at[0, chip],
+            mate_ep,
+            tp,
+        ).start()
+
+    @pl.when(core == 1)
+    def _():
+        pair_copy(1, chip).start()
 
     own_rows = residual[:, :part]
     for t in range(1, splits):
         own_rows = jnp.where(tp == t, residual[:, t * part : (t + 1) * part], own_rows)
     own_ref[...] = own_rows
 
-    def collect(first, last):
+    def collect(of, first, last):
         for i in range(first, last):
             slot = source(chip, i, chips)
-            feat_copy(i, slot).wait_recv()
-            pair_copy(slot).start()
-
-    collect(1, chips // 2)
+            feat_copy(i, of, slot).wait_recv()
+            pair_copy(of, slot).start()
+
+    @pl.when(core == 1)
+    def _():
+        collect(1, 1, chips // 2)
+
     dense_all.wait_recv()
     if fold > 1:
         for s in range(peers):
@@ -495,9 +539,18 @@
         dense_weights = dense[...]
     else:
         dense_weights = arrived[...].reshape(width, arrived.shape[2])
-    collect(chips // 2, chips)
+    @pl.when(core == 1)
+    def _():
+        collect(1, chips // 2, chips)
+        feat_copy(1, 0, chip).wait_recv()
+        collect(0, 1, chips)
+
+    @pl.when(core == 0)
+    def _():
+        batch(features.at[1], 3, 2).wait_recv()
+
     pltpu.make_async_copy(gate_up, gate_up, load_sem.at[5]).wait()
-    loads[7].wait()
+    expert_loads[2].wait()
     rows_of = chips * seqs
     branch_row = branch_ref[...].astype(jnp.float32).reshape(1, width)
 
@@ -525,10 +578,14 @@
             preferred_element_type=jnp.float32,
         )
 
-    half_out[...] = feed_forward(core).astype(jnp.bfloat16)
+    half_out[...] = feed_forward(1 - core).astype(jnp.bfloat16)
     half_copy.start()
-    pairs_all.wait_recv()
-    total = feed_forward(mate)
+
+    @pl.when(core == 0)
+    def _():
+        batch(features.at[0, others], 3, 1).wait_recv()
+
+    total = feed_forward(core)
     half_copy.wait_recv()
     total = total + half_in[...].astype(jnp.float32)
     for t in range(splits):
@@ -537,12 +594,23 @@
         )
     for i in reversed(range(chips)):
         for j in reversed(range(splits)):
-            ret_copy(i, j).start()
+            if i or j:
+                ret_copy(i, j).start()
+    returned[chip * splits + tp] = packed[tp, chip]
 
     parts_out.wait_send()
     dense_all.wait_send()
-    feats_out.wait_send()
-    pairs_all.wait_send()
+
+    @pl.when(core == 0)
+    def _():
+        batch(features.at[0], 2, 1).wait_send()
+
+    @pl.when(core == 1)
+    def _():
+        batch(features.at[0, others], 2, 1).wait_send()
+        batch(features.at[0, others], 3, 1).wait_send()
+        batch(features.at[1], 3, 1).wait_send()
+
     half_copy.wait_send()
     rets_all.wait_recv()
     rets_all.wait_send()
@@ -670,8 +738,8 @@
             dma(seqs // 2),
             dma(6),
             dma(splits),
-            dma(chips),
-            dma(4),
+            pltpu.SemaphoreType.DMA((cores, chips)),
+            dma(5),
         ],
         compiler_params=pltpu.CompilerParams(
             collective_id=0, has_side_effects=True, vmem_limit_bytes=40 * 2**20

time: 27.6 us -> 26.6 us (0.964)
  Pallas kernels: 26.7 us -> 25.8 us
    pallas_call x1, Pallas kernels: 24.7 us -> 23.7 us  [body(): pl.pallas_call(functools.partial(layer_kernel, peers, splits, share, fold...]
where the time goes in v3:
time: 26.6 us; the launch traced here: 26.4 us
  Pallas kernels  25.8 us (97%)
  between operations  0.65 us (2%)
    pallas_call x1, Pallas kernels, body(): pl.pallas_call(functools.partial(layer_kernel, peers, splits, share, fold...  23.7 us
    pallas_call x1, Pallas kernels, body(): pl.pallas_call(finish_kernel, out_shape=(shape((seqs, part), bf16), shape...  2.06 us

profile of v3, /device:TPU:0, one launch (start us, length us, event | category | flops | bytes accessed | tf_op | source)
XLA Modules:
  0.0 26.4 jit_solution(9314788814874613773)
XLA Ops:
  0.6 23.7 %shard_map.308 = (f32[8,512]{1,0:T(8,128)S(1)}, bf16[16,8,512]{2,1,0:T(8,128)(2,1)S(1)}, f32[8,16,64,128]{3,2,1,0:T(8,128)S(1)}, bf16[3,8,1024]{2,1,0:T(8,128)(2...) custom-call(bf16[8,1024]{1,0:T(8,128)(2,1)} %tokens_hbm.1, f32[1,1024]{1,0:T(1,128)} %bitcast.19, ...), custom_call_target="tpu_custom_call" | custom-call | flops 1000000000 | bytes 20000000 | tf_op jit(solution)/shard_map/pallas_call | solution.py:689
  24.3 2.1 %shard_map.309 = (bf16[8,512]{1,0:T(8,128)(2,1)}, f32[8,16,64,128]{3,2,1,0:T(8,128)}, bf16[3,8,1024]{2,1,0:T(8,128)(2,1)}, bf16[3,8,512]{2,1,0:T(8,128)(2,1)}, bf16[3,8,512]{2,1,0:T(8,128)(2,1)}) custom-call(f32[8,512]{1,0:T(8,128)S(1)} %get-tuple-element.16.own_ref, bf16[16,8,512]{2,1,0:T(8,128)(2,1)S(1)} %get-tuple-element.17.returned, ...), custom_call_target="tpu_custom_call" | custom-call | flops 100000 | bytes 5000000 | tf_op jit(solution)/shard_map/pallas_call | solution.py:781

commit v4 on v3

--- a/solution.py
+++ b/solution.py
@@ -409,7 +409,6 @@
                 copy.start()
         if s0 == 0:
             meet_and_send(2)
-        if s0 == seqs // 2:
             meet_and_send(1)
         fetch_state[s0 // 2].wait()
         for g in range(groups):

time: 26.6 us -> 26.6 us (level)
  no operation moved by 1% of the time
where the time goes in v4:
time: 26.6 us; the launch traced here: 26.4 us
  Pallas kernels  25.8 us (97%)
  between operations  0.65 us (2%)
    pallas_call x1, Pallas kernels, body(): pl.pallas_call(functools.partial(layer_kernel, peers, splits, share, fold...  23.7 us
    pallas_call x1, Pallas kernels, body(): pl.pallas_call(finish_kernel, out_shape=(shape((seqs, part), bf16), shape...  2.06 us

profile of v4, /device:TPU:0, one launch (start us, length us, event | category | flops | bytes accessed | tf_op | source)
XLA Modules:
  0.0 26.4 jit_solution(15282261148709987653)
XLA Ops:
  0.6 23.7 %shard_map.308 = (f32[8,512]{1,0:T(8,128)S(1)}, bf16[16,8,512]{2,1,0:T(8,128)(2,1)S(1)}, f32[8,16,64,128]{3,2,1,0:T(8,128)S(1)}, bf16[3,8,1024]{2,1,0:T(8,128)(2...) custom-call(bf16[8,1024]{1,0:T(8,128)(2,1)} %tokens_hbm.1, f32[1,1024]{1,0:T(1,128)} %bitcast.19, ...), custom_call_target="tpu_custom_call" | custom-call | flops 1000000000 | bytes 20000000 | tf_op jit(solution)/shard_map/pallas_call | solution.py:688
  24.3 2.1 %shard_map.309 = (bf16[8,512]{1,0:T(8,128)(2,1)}, f32[8,16,64,128]{3,2,1,0:T(8,128)}, bf16[3,8,1024]{2,1,0:T(8,128)(2,1)}, bf16[3,8,512]{2,1,0:T(8,128)(2,1)}, bf16[3,8,512]{2,1,0:T(8,128)(2,1)}) custom-call(f32[8,512]{1,0:T(8,128)S(1)} %get-tuple-element.16.own_ref, bf16[16,8,512]{2,1,0:T(8,128)(2,1)S(1)} %get-tuple-element.17.returned, ...), custom_call_target="tpu_custom_call" | custom-call | flops 100000 | bytes 5000000 | tf_op jit(solution)/shard_map/pallas_call | solution.py:780
